TPU v7x, 512 devices: a whole 4x4x16 slice. The times are simulated.
512 devices in a mesh: tp: 64 (over z, y), dp: 8 (over x, core).
Axes of the slice: x: 4, y: 4, z: 16, core: 2. Of those that a mesh axis runs over, the one named last changes fastest.
Arguments:
- tokens: bfloat16 [192, 4096], P('tp', 'dp'), may hold values from -6 to 6
- lengths: int32 [48], P('dp'), may hold values from 1 to 4, 84 in all
- norm_gain: float32 [2, 4096], P(None, 'dp'), may hold values from 0.1 to 1.9
- gate_weight: bfloat16 [2, 4096, 8192], P(None, 'dp', 'tp'), may hold values from -0.09375 to 0.09375
- value_weight: bfloat16 [2, 4096, 8192], P(None, 'dp', 'tp'), may hold values from -0.09375 to 0.09375
- vector_weight: bfloat16 [2, 4096, 2, 2048], P(None, 'dp', None, 'tp'), may hold values from -0.09375 to 0.09375
- step_weight: bfloat16 [2, 4096, 128], P(None, 'dp'), may hold values from -0.09375 to 0.09375
- step_bias: float32 [2, 128], P(None, 'tp'), may hold values from -3 to 0
- decay_rate: float32 [2, 128], P(None, 'tp'), may hold values from 0.003 to 1
- value_taps: bfloat16 [2, 4, 8192], P(None, None, 'tp'), may hold values from -3 to 3
- vector_taps: bfloat16 [2, 4, 2, 2048], P(None, None, None, 'tp'), may hold values from -3 to 3
- out_weight: bfloat16 [2, 8192, 4096], P(None, 'tp', 'dp'), may hold values from -0.0625 to 0.0625
- recurrent_state: float32 [2, 48, 128, 64, 128], P(None, 'dp', 'tp'), may hold values from -4 to 4
- value_history: bfloat16 [2, 48, 3, 8192], P(None, 'dp', None, 'tp'), may hold values from -6 to 6
- vector_history: bfloat16 [2, 48, 3, 2, 2048], P(None, 'dp', None, None, 'tp'), may hold values from -6 to 6
Outputs:
- next_tokens: bfloat16 [192, 4096], P('tp', 'dp')
- next_state: float32 [2, 48, 128, 64, 128], P(None, 'dp', 'tp')
- next_value_history: bfloat16 [2, 48, 3, 8192], P(None, 'dp', None, 'tp')
- next_vector_history: bfloat16 [2, 48, 3, 2, 2048], P(None, 'dp', None, None, 'tp')
Inputs may be any that keep to these rules, and one draw needn't show every extreme that they name: `lengths`: the number of live new tokens of each sequence; some sequences have more than twice the mean.
All inputs are finite; a program needn't handle non-finite values. No bound on the sum of `lengths` on one device may be relied on, other than what follows from the above.
Results may differ from a plain program's by a relative error of at most 0.029.
Values may be sent and summed in bfloat16 or wider, within the bound.
No kernel may reach another device: no remote copies, remote signals or barrier semaphores. Data moves between devices by JAX's collectives and lax.ppermute only.
A program may use at most 64 MiB of HBM per device.

v0:
```python
import functools

import jax
import jax.numpy as jnp
from jax import lax
from jax.experimental import pallas as pl
from jax.experimental.pallas import tpu as pltpu
from jax.sharding import Mesh, PartitionSpec as P

D = 4096
HEADS = 128
HEAD_DIM = 64
GROUPS = 16
CONV = 4
NEW = 4
LAYERS = 2
norm_floor = 0.1

ZN, YN, DN = 16, 4, 8
SEQ = 6
bf16 = jnp.bfloat16
f32 = jnp.float32
COLS = 640


def exchange(pieces, axis):
    return lax.all_to_all(pieces, axis, 0, 0, tiled=True)


def copies(value, peers):
    return jnp.broadcast_to(value[None], (peers, *value.shape))


def one_hot(rows, cols, target):
    row = lax.broadcasted_iota(jnp.int32, (rows, cols), 0)
    col = lax.broadcasted_iota(jnp.int32, (rows, cols), 1)
    return jnp.where(row == target(col), 1.0, 0.0).astype(bf16)


def mm(a, b):
    return lax.dot_general(a, b, (((1,), (0,)), ((), ())), preferred_element_type=f32)


def mm_t(a, b):
    return lax.dot_general(a, b, (((1,), (1,)), ((), ())), preferred_element_type=f32)


def normed_rows(rows, gain):
    widened = rows.astype(f32)
    squares = jnp.sum(widened * widened, axis=1, keepdims=True)
    return (widened * gain).astype(bf16), squares


def square_lane():
    return (8 * lax.axis_index("z") + 64) % HEADS


def step_lanes(normed, squares, step_w):
    step = mm(normed, step_w)
    lane = lax.broadcasted_iota(jnp.int32, step.shape, 1)
    return jnp.where(lane == square_lane(), squares, step)


def first_projection(plane_ref, misc_ref, weight_ref, out_ref):
    plane = plane_ref[...].reshape(512, 512)

    def token_source(col):
        i = col % 8
        return jnp.where(i < 3, 12 * ((col // 8) % ZN) + 3 * (col // 128) + i, -1)

    def vector_source(col):
        j = col % 8 - 4
        n = 8 * ((col // 8) % ZN) + 2 * (col // 128) + j % 2
        return jnp.where((j >= 0) & (j < 4), 128 * (j // 2) + n, -1)

    rows = mm(one_hot(192, 512, token_source), plane).astype(bf16)
    vector_w = mm(one_hot(256, 512, vector_source), plane).astype(bf16)
    normed, squares = normed_rows(rows, gain_row(misc_ref, 0))
    parts = [
        mm(normed, weight_ref[:, 0:128]),
        mm(normed, weight_ref[:, 128:256]),
        mm_t(normed, vector_w),
        step_lanes(normed, squares, weight_ref[:, 256:384]),
    ]
    at = 0
    for part in parts:
        width = part.shape[1]
        out_ref[:, :, at : at + width] = part.astype(bf16).reshape(DN, 24, width)
        at += width


def second_projection(rows_ref, misc_ref, step_ref, w0, w1, w2, w3, out_ref):
    y = lax.axis_index("y")
    normed, squares = normed_rows(rows_ref[...], gain_row(misc_ref, 1))
    pieces = [w0, w1, w2, w3]

    def source(col):
        j = col % 4
        n = 8 * ((col // 4) % ZN) + 2 * ((y - col // 64) % YN) + j % 2
        return 128 * (j // 2) + n

    stacked = jnp.concatenate(
        [
            jnp.concatenate([w[1024 + 64 * b : 1088 + 64 * b] for b in range(4)], axis=1)
            for w in pieces
        ],
        axis=0,
    )
    vector_w = mm(one_hot(256, 256, source), stacked).astype(bf16)
    vector = mm_t(normed, vector_w).astype(bf16)
    extra = step_lanes(normed, squares, step_ref[0]).astype(bf16)
    for k, w in enumerate(pieces):
        to = (y - k) % YN
        for n in range(2):
            total = mm(normed, w[512 * n : 512 * n + 512])
            out_ref[to, :, 128 * n : 128 * n + 128] = total.astype(bf16)
        out_ref[to, :, 256:512] = vector
        out_ref[to, :, 512:640] = extra


def out_projection(mixed_ref, w0, w1, w2, w3, *rest, first_row):
    y = lax.axis_index("y")
    total = jnp.zeros((64, 512), f32)
    for k, w in enumerate([w0, w1, w2, w3]):
        total += mm(mixed_ref[(y - k) % YN], w[first_row : first_row + 128])
    if len(rest) == 1:
        rest[0][...] = total.astype(bf16).reshape(ZN, 4, 512)
        return
    returned_ref, out_ref = rest
    returned = jnp.concatenate(
        [returned_ref[:, 0:128], returned_ref[:, 128:256], jnp.zeros((32, 128), bf16)], axis=0
    )
    slot = one_hot(64, ZN, lambda col: 4 * col + 3)
    halves = []
    for nl in range(2):
        row = lax.broadcasted_iota(jnp.int32, (ZN, 128), 0)
        col = lax.broadcasted_iota(jnp.int32, (ZN, 128), 1)
        chosen = jnp.where(col == 8 * row + 2 * y + nl, 1.0, 0.0).astype(bf16)
        halves.append(mm_t(chosen, returned).astype(bf16))
    tail = jnp.concatenate(halves, axis=1)
    left = (total[:, 0:256] + mm(slot, tail)).astype(bf16)
    whole = jnp.concatenate([left, total[:, 256:512].astype(bf16)], axis=1)
    out_ref[...] = whole.reshape(ZN, 4, 512)


def row_col(shape):
    return (
        lax.broadcasted_iota(jnp.int32, shape, 0),
        lax.broadcasted_iota(jnp.int32, shape, 1),
    )


def silu(x):
    return x * jax.nn.sigmoid(x)


def place_first(col):
    return 8 * (col % NEW) + col // NEW


def place_second(col):
    i = col % 4
    n = 12 * ((col // 4) % 2) + 3 * (col // 8) + i
    return jnp.where(i < 3, 8 * (n % NEW) + n // NEW, -1)


def conv(old, taps, fresh):
    rows = old + [fresh[8 * t : 8 * t + 8] for t in range(NEW)]
    return [silu(sum(rows[t + k] * taps[k] for k in range(CONV))) for t in range(NEW)]


def old_values(misc_ref, layer):
    return [misc_ref[32 * layer + 8 * k : 32 * layer + 8 * k + 8] for k in range(CONV - 1)]


def old_vectors(vhist_ref, layer):
    return [vhist_ref[layer, k].astype(f32) for k in range(CONV - 1)]


def setup(
    len_ref,
    gain_hbm,
    bias_hbm,
    rate_hbm,
    taps_hbm,
    history_hbm,
    gate_hbm,
    value_hbm,
    misc_ref,
    base_ref,
    gain_ref,
    bias_ref,
    rate_ref,
    taps_ref,
    history_ref,
    sems,
):
    pairs = (
        (gain_hbm, gain_ref),
        (bias_hbm, bias_ref),
        (rate_hbm, rate_ref),
        (taps_hbm, taps_ref),
        (history_hbm, history_ref),
        (gate_hbm.at[1], base_ref.at[0:512]),
        (value_hbm.at[1], base_ref.at[512:1024]),
    )
    moves = [pltpu.make_async_copy(a, b, sems.at[n]) for n, (a, b) in enumerate(pairs)]
    for move in moves:
        move.start()
    row, lane = row_col((8, 128))
    lens = jnp.zeros((8, 128), f32)
    for s in range(SEQ):
        lens = jnp.where(row == s, len_ref[s].astype(f32), lens)
    misc_ref[0:64] = jnp.zeros((64, 128), f32)
    misc_ref[64:72] = lens
    misc_ref[72:80] = jnp.zeros((8, 128), f32)
    for move in moves:
        move.wait()
    left = lane[0:1] < HEAD_DIM
    for layer in range(LAYERS):
        for n, ref in enumerate((bias_ref, rate_ref)):
            both = jnp.where(left, ref[layer : layer + 1, 0:1], ref[layer : layer + 1, 1:2])
            misc_ref[72 + 2 * layer + n : 73 + 2 * layer + n] = both
        for b in range(4):
            part = gain_ref[layer : layer + 1, 128 * b : 128 * b + 128]
            misc_ref[80 + 4 * layer + b : 81 + 4 * layer + b] = part
        for k in range(CONV - 1):
            at = 32 * layer + 8 * k
            for s in range(SEQ):
                misc_ref[at + s : at + s + 1] = history_ref[s, k, layer : layer + 1].astype(f32)
        at = 32 * layer + 24
        misc_ref[at : at + CONV] = taps_ref[layer].astype(f32)


def gain_row(misc_ref, layer):
    parts = [misc_ref[80 + 4 * layer + b : 81 + 4 * layer + b] for b in range(4)]
    return jnp.concatenate(parts, axis=1)


def prepare(
    token_hbm,
    weight_hbm,
    history_hbm,
    taps_hbm,
    out_ref,
    token_ref,
    weight_ref,
    history_ref,
    taps_ref,
    stack_ref,
    sems,
):
    moves = [
        pltpu.make_async_copy(source, target, sems.at[n])
        for n, (source, target) in enumerate(
            (
                (history_hbm, history_ref),
                (taps_hbm, taps_ref),
                (token_hbm, token_ref),
                (weight_hbm, weight_ref),
            )
        )
    ]
    for move in moves:
        move.start()
    for move in moves[:3]:
        move.wait()
    stack_ref[...] = jnp.zeros((128, 32), f32)
    at = 0
    for layer in range(LAYERS):
        for s in range(SEQ):
            for k in range(CONV - 1):
                stack_ref[at : at + 2] = history_ref[layer, s, k].astype(f32)
                at += 2
    for layer in range(LAYERS):
        for k in range(CONV):
            stack_ref[at : at + 2] = taps_ref[layer, k].astype(f32)
            at += 2
    turned = jnp.transpose(stack_ref[...])
    tokens = jnp.concatenate([token_ref[...].astype(f32), jnp.zeros((1, 512), f32)], axis=0)
    row, _ = row_col((4, 512))
    for g in range(GROUPS):
        both = [turned[g : g + 1], turned[GROUPS + g : GROUPS + g + 1], jnp.zeros((1, 256), f32)]
        tail = jnp.broadcast_to(jnp.concatenate(both, axis=1), (4, 512))
        out_ref[g, 0] = jnp.where(row == 3, tail, tokens).astype(bf16)

    def source(col):
        c = col % 32
        return 4 * (c % GROUPS) + 2 * (col // 32) + c // GROUPS

    order = one_hot(64, 64, source)
    moves[3].wait()
    for layer in range(LAYERS):
        cols = weight_ref[layer].reshape(64, 512)
        out_ref[:, 1 + layer] = mm(order, cols).astype(bf16).reshape(GROUPS, 4, 512)


def unpack(plane_ref, vhist_ref, vtaps_ref):
    def source(col):
        return jnp.where(col % 8 == 3, 4 * ((col // 8) % ZN) + col // 128, -1)

    small = mm(one_hot(64, 512, source), plane_ref[:, :, 0:256].reshape(512, 256))
    spread = jnp.zeros((128, 128), f32)
    row, col = row_col((64, 128))
    for nl in range(2):
        turned = jnp.transpose(small[:, 128 * nl : 128 * nl + 128]).astype(bf16)
        spread += mm(turned, jnp.where(col == 2 * row + nl, 1.0, 0.0).astype(bf16))

    def order(m):
        kind = m // 2
        old = 24 * (2 * (m // 36) + m % 2) + 8 * (kind % 3) + (kind // 3) % SEQ
        tap = 96 + 8 * (2 * ((m - 72) // 8) + m % 2) + (kind - 36) % CONV
        return jnp.where(m < 72, old, jnp.where(m < 88, tap, -1))

    rows = mm(one_hot(128, 128, order), spread.astype(bf16)).astype(bf16)
    for layer in range(LAYERS):
        for rw in range(2):
            lanes = slice(128 * rw, 128 * rw + 128)
            for k in range(CONV - 1):
                at = 24 * (2 * layer + rw) + 8 * k
                vhist_ref[layer, k, :, lanes] = rows[at : at + 8]
            at = 96 + 8 * (2 * layer + rw)
            vtaps_ref[layer, :, lanes] = rows[at : at + 8]


def middle(
    part_ref,
    misc_ref,
    vhist_ref,
    vtaps_ref,
    state_ref,
    msg_ref,
    keep_ref,
    write_ref,
    decay_ref,
    fresh_ref,
    *,
    layer,
):
    if layer == 0:
        total = sum(part_ref[d].astype(f32) for d in range(DN))
        place = one_hot(32, 24, place_first)
    else:
        rows = [sum(part_ref[y, d].astype(f32) for d in range(DN)) for y in range(YN)]
        total = jnp.concatenate(rows, axis=0)
        place = one_hot(32, 32, place_second)
    tail = total[:, 512:640]
    _, lane = row_col(tail.shape)
    squares = jnp.sum(jnp.where(lane == square_lane(), tail, 0.0), axis=1, keepdims=True)
    scaled = (total * lax.rsqrt(squares / D + norm_floor)).astype(bf16)
    rows = mm(place, scaled)
    fresh_ref[...] = rows[:, 128:512].astype(bf16)
    gate = rows[:, 0:128]

    head = 8 * lax.axis_index("z") + 2 * lax.axis_index("y")
    tail = rows[:, 512:640]
    _, lane = row_col(tail.shape)
    first = jnp.sum(jnp.where(lane == head, tail, 0.0), axis=1, keepdims=True)
    second = jnp.sum(jnp.where(lane == head + 1, tail, 0.0), axis=1, keepdims=True)
    left = lane < HEAD_DIM
    at = 72 + 2 * layer
    raw = jnp.where(left, first, second) + misc_ref[at : at + 1]
    rate = misc_ref[at + 1 : at + 2]
    soft = jnp.maximum(raw, 0.0) + jnp.log1p(jnp.exp(-jnp.abs(raw)))
    lens = misc_ref[64:72, 0:1]
    live = [jnp.where(lens > t, 1.0, 0.0) for t in range(NEW)]
    step = [soft[8 * t : 8 * t + 8] * live[t] for t in range(NEW)]
    cumulative = []
    for t in range(NEW):
        grown = step[t] * rate
        cumulative.append(grown if t == 0 else cumulative[-1] + grown)

    at = 32 * layer + 24
    taps = [misc_ref[at + k : at + k + 1] for k in range(CONV)]
    values = conv(old_values(misc_ref, layer), taps, rows[:, 128:256])
    taps = [vtaps_ref[layer, k : k + 1].astype(f32) for k in range(CONV)]
    vectors = conv(old_vectors(vhist_ref, layer), taps, rows[:, 256:512])
    write = [v[:, 0:128] for v in vectors]
    read = [v[:, 128:256] for v in vectors]
    stepped = [values[t] * step[t] for t in range(NEW)]

    reads = jnp.concatenate(read, axis=0).astype(bf16)
    row, _ = row_col((32, 128))
    carried = jnp.zeros((32, 128), f32)
    for s in range(SEQ):
        carried = jnp.where(row % 8 == s, mm_t(reads, state_ref[0, s].astype(bf16)), carried)

    mixed = []
    for t in range(NEW):
        y = jnp.exp(-cumulative[t]) * carried[8 * t : 8 * t + 8]
        for u in range(t + 1):
            score = jnp.sum(read[t] * write[u], axis=1, keepdims=True)
            y = y + score * jnp.exp(cumulative[u] - cumulative[t]) * stepped[u]
        mixed.append(y * silu(gate[8 * t : 8 * t + 8]) * live[t])
    mixed = jnp.concatenate(mixed, axis=0).astype(bf16)
    row, col = row_col((32, 32))
    i = row % 4
    n = 12 * ((row // 4) % 2) + 3 * (row // 8) + i
    pick = (col == 8 * (n % NEW) + n // NEW) & (i < 3)
    ordered = mm(jnp.where(pick, 1.0, 0.0).astype(bf16), mixed).astype(bf16)
    for y in range(YN):
        for d in range(DN):
            msg_ref[y * DN + d] = ordered[8 * y : 8 * y + 8]

    last = cumulative[-1]
    for t in range(NEW):
        keep_ref[8 * t : 8 * t + 8] = jnp.exp(cumulative[t] - last) * stepped[t]
        write_ref[8 * t : 8 * t + 8] = write[t]
    decay_ref[...] = jnp.exp(-last)


def finish(
    misc_ref,
    keep_ref,
    write_ref,
    decay_ref,
    fresh_ref,
    vhist_ref,
    state_ref,
    *rest,
    layer,
):
    next_ref, value_ref, vector_ref = rest[-3:]
    kept = jnp.transpose(keep_ref[...])
    _, col = row_col(kept.shape)
    write = write_ref[...].astype(bf16)
    for s in range(SEQ):
        fresh = mm(jnp.where(col % 8 == s, kept, 0.0).astype(bf16), write)
        for h in range(2):
            at = slice(HEAD_DIM * h, HEAD_DIM * h + HEAD_DIM)
            decay = decay_ref[s : s + 1, HEAD_DIM * h : HEAD_DIM * h + 1]
            next_ref[0, s, at] = state_ref[0, s, at] * decay + fresh[at]
    lens = misc_ref[64:72, 0:1]
    for out_ref, old, lo, hi in (
        (value_ref, old_values(misc_ref, layer), 0, 128),
        (vector_ref, old_vectors(vhist_ref, layer), 128, 384),
    ):
        rows = old + [fresh_ref[8 * t : 8 * t + 8, lo:hi].astype(f32) for t in range(NEW)]
        for k in range(CONV - 1):
            chosen = rows[k + 1]
            for r in range(k + 2, k + NEW + 1):
                chosen = jnp.where(lens + k == r, rows[r], chosen)
            out_ref[k] = chosen.astype(bf16)


def call(kernel, shapes, *args):
    vmem = pl.BlockSpec(memory_space=pltpu.VMEM)
    outs = [jax.ShapeDtypeStruct(shape, dtype) for shape, dtype in shapes]
    results = pl.pallas_call(
        kernel,
        out_shape=outs,
        in_specs=[vmem] * len(args),
        out_specs=[vmem] * len(outs),
        compiler_params=pltpu.CompilerParams(vmem_limit_bytes=12 << 20),
    )(*args)
    return results[0] if len(outs) == 1 else results


def ending(update_ref, token_ref, out_ref, vector_ref):
    total = sum(update_ref[z].astype(f32) for z in range(ZN))
    out_ref[...] = (total[0:3] + token_ref[...].astype(f32)).astype(bf16)
    rows = [update_ref[z, 3:4, 0:256].astype(f32) for z in range(ZN)]
    rows = jnp.concatenate(rows, axis=0)
    both = jnp.concatenate(
        [jnp.transpose(rows[:, 0:128]), jnp.transpose(rows[:, 128:256])], axis=1
    )
    for layer in range(LAYERS):
        for k in range(CONV - 1):
            for s in range(SEQ):
                at = 24 * layer + 8 * k + s
                pair = jnp.concatenate([both[at : at + 1], both[48 + at : 49 + at]], axis=0)
                vector_ref[layer, s, k] = pair.astype(bf16)


def close(layer, *args):
    vmem = pl.BlockSpec(memory_space=pltpu.VMEM)
    block = pl.BlockSpec((1, SEQ, 128, 128), lambda i: (layer, 0, 0, 0))
    space = [vmem] * 7 + [pl.BlockSpec(memory_space=pl.ANY)] * (len(args) - 7)
    return pl.pallas_call(
        functools.partial(finish, layer=layer),
        grid=(1,),
        out_shape=[
            jax.ShapeDtypeStruct((LAYERS, SEQ, 128, 128), f32),
            jax.ShapeDtypeStruct((3, 8, 128), bf16),
            jax.ShapeDtypeStruct((3, 8, 256), bf16),
        ],
        in_specs=space,
        out_specs=[block, vmem, vmem],
        input_output_aliases={7: 0} if layer else {},
        compiler_params=pltpu.CompilerParams(vmem_limit_bytes=12 << 20),
    )(*args)


def from_y(value, k):
    return lax.ppermute(value, "y", [(i, (i + k) % YN) for i in range(YN)])


def body(
    tokens,
    lengths,
    norm_gain,
    gate_weight,
    value_weight,
    vector_weight,
    step_weight,
    step_bias,
    decay_rate,
    value_taps,
    vector_taps,
    out_weight,
    recurrent_state,
    value_history,
    vector_history,
):
    first = pl.pallas_call(
        prepare,
        out_shape=jax.ShapeDtypeStruct((ZN, 3, 4, 512), bf16),
        in_specs=[pl.BlockSpec(memory_space=pltpu.MemorySpace.HBM)] * 4,
        out_specs=pl.BlockSpec(memory_space=pltpu.VMEM),
        scratch_shapes=[
            pltpu.VMEM((3, 512), bf16),
            pltpu.VMEM((2, 2, 32, 512), bf16),
            pltpu.VMEM((2, SEQ, 3, 2, 32), bf16),
            pltpu.VMEM((2, CONV, 2, 32), bf16),
            pltpu.VMEM((128, 32), f32),
            pltpu.SemaphoreType.DMA((4,)),
        ],
    )(tokens, vector_weight.transpose(0, 2, 3, 1), vector_history, vector_taps)
    first, outs, lens = lax.optimization_barrier(
        (first, out_weight.reshape(256, 512), lengths)
    )
    first = exchange(first, "z")
    early = jnp.concatenate([gate_weight[0], value_weight[0], step_weight[0]], axis=1)
    out_2 = from_y(outs, 2)
    out_3 = from_y(outs, 3)
    misc, base = pl.pallas_call(
        setup,
        out_shape=[jax.ShapeDtypeStruct((88, 128), f32), jax.ShapeDtypeStruct((1280, 128), bf16)],
        in_specs=[pl.BlockSpec(memory_space=pltpu.SMEM)]
        + [pl.BlockSpec(memory_space=pltpu.MemorySpace.HBM)] * 7,
        out_specs=[pl.BlockSpec(memory_space=pltpu.VMEM)] * 2,
        scratch_shapes=[
            pltpu.VMEM((2, 512), f32),
            pltpu.VMEM((2, 2), f32),
            pltpu.VMEM((2, 2), f32),
            pltpu.VMEM((2, CONV, 128), bf16),
            pltpu.VMEM((SEQ, 3, 2, 128), bf16),
            pltpu.SemaphoreType.DMA((7,)),
        ],
    )(
        lens,
        norm_gain,
        step_bias,
        decay_rate,
        value_taps,
        value_history.transpose(1, 2, 0, 3),
        gate_weight,
        value_weight,
    )
    plane = exchange(copies(first[:, :2], YN), "y").reshape(128, 4, 512)
    out_1 = from_y(outs, 1)
    outs = [outs, out_1, out_2, out_3]
    blocks = first[:, 2].reshape(64, 4, 128).transpose(1, 0, 2).reshape(256, 128)
    later = lax.dynamic_update_slice(base, blocks, (1024, 0))
    vhist, vtaps = call(unpack, [((2, 3, 8, 256), bf16), ((2, 8, 256), bf16)], plane)

    def mid(part, layer, old, *done):
        msg, keep, write, decay, fresh = call(
            functools.partial(middle, layer=layer),
            [
                ((YN * DN, 8, 128), bf16),
                ((32, 128), f32),
                ((32, 128), f32),
                ((8, 128), f32),
                ((32, 384), bf16),
            ],
                        part,
            misc,
            vhist,
            vtaps,
            old,
        )
        after = close(layer, misc, keep, write, decay, fresh, vhist, old, *done)
        msg = exchange(msg, ("y", "dp"))
        return msg.reshape(YN, DN * 8, 128), after

    part = call(
        first_projection,
        [((DN, 24, COLS), bf16)],
                plane,
        misc,
        early,
    )
    old = recurrent_state[:1]
    part = exchange(part, "dp")
    later_2 = from_y(later, 2)
    mixed, (state, value0, vector0) = mid(part, 0, old.reshape(1, SEQ, 128, 128))
    later_3 = from_y(later, 3)
    update = call(
        functools.partial(out_projection, first_row=0),
        [((ZN, 4, 512), bf16)],
                mixed,
        *outs,
    )
    update = exchange(update, "z")
    later_1 = from_y(later, 1)
    update = jnp.sum(update.astype(f32), axis=0)[:3]
    token_rows = (tokens.astype(f32) + update).astype(bf16)
    quarter = copies(jnp.pad(token_rows, ((0, 1), (0, 0))), ZN)
    quarter, old = lax.optimization_barrier((quarter, recurrent_state))
    quarter = exchange(quarter, "z").reshape(64, 512)
    old = old[1:].reshape(1, SEQ, 128, 128)
    later = [later, later_1, later_2, later_3]
    part = call(
        second_projection,
        [((YN, 64, COLS), bf16)],
                quarter,
        misc,
        step_weight[1:],
        *later,
    )
    part = exchange(part.reshape(YN * DN, 8, COLS), ("y", "dp")).reshape(YN, DN, 8, COLS)
    mixed, (state, value1, vector1) = mid(part, 1, old, state)
    update = call(
        functools.partial(out_projection, first_row=128),
        [((ZN, 4, 512), bf16)],
                mixed,
        *outs,
        jnp.concatenate([vector0, vector1], axis=0).reshape(48, 256),
    )
    update = exchange(update, "z")
    token_rows, next_vector = call(
        ending,
        [((3, 512), bf16), ((LAYERS, SEQ, CONV - 1, 2, 32), bf16)],
        update,
        token_rows,
    )
    return (
        token_rows,
        state.reshape(recurrent_state.shape),
        jnp.stack([value0, value1])[:, :, :SEQ].transpose(0, 2, 1, 3),
        next_vector,
    )


def solution(mesh):
    grid = Mesh(mesh.devices.reshape(ZN, YN, DN), ("z", "y", "dp"))
    tp = ("z", "y")

    return jax.shard_map(
        body,
        mesh=grid,
        in_specs=(
            P(tp, "dp"),
            P("dp"),
            P(None, "dp"),
            P(None, "dp", tp),
            P(None, "dp", tp),
            P(None, "dp", None, tp),
            P(None, "dp", None),
            P(None, tp),
            P(None, tp),
            P(None, None, tp),
            P(None, None, None, tp),
            P(None, tp, "dp"),
            P(None, "dp", tp, None, None),
            P(None, "dp", None, tp),
            P(None, "dp", None, None, tp),
        ),
        out_specs=(
            P(tp, "dp"),
            P(None, "dp", tp, None, None),
            P(None, "dp", None, tp),
            P(None, "dp", None, None, tp),
        ),
        check_vma=False,
    )
```

profile of v0, /device:TPU:1, one launch (start us, length us, event | category | flops | bytes accessed | tf_op | source)
XLA Modules:
  0.0 167.4 jit_solution(11727774995444359282)
XLA Ops:
  0.6 1.8 %shard_map.174 = bf16[16,3,4,512]{3,2,1,0:T(4,128)(2,1)} custom-call(bf16[3,512]{1,0:T(4,128)(2,1)} %token_hbm.1, bf16[2,2,32,512]{3,2,1,0:T(8,128)(2,1)} %bitcast.44, bf16[2,6,3,2,32]{4,3,2,1,0:T(2,128)(2,1)} %history_hbm.1, bf16[2,4,2,32]{3,2,1,0:T(2,128)(2,1)} %taps_hbm.2), custom_call_target="tpu_custom_call" | custom-call | tf_op jit(solution)/shard_map/pallas_call | solution.py:515
  2.5 28.2 %all_to_all.45 = bf16[16,3,4,512]{3,2,1,0:T(4,128)(2,1)S(1)} all-to-all(bf16[16,3,4,512]{3,2,1,0:T(4,128)(2,1)} %shard_map.174), channel_id=1, replica_groups=mesh['z'=16,'y'=4,'dp'=8] {'z'}, dimensions={0} | all-to-all | bytes 393216 | tf_op jit(solution)/shard_map/all_to_all | solution.py:27
  31.7 4.3 %all-to-all-start.1 = ((bf16[4,16,2,4,512]{4,3,2,1,0:T(4,128)(2,1)}), bf16[4,16,2,4,512]{4,3,2,1,0:T(4,128)(2,1)S(1)}, u32[]{:S(2)}, u32[]{:S(2)}) async-start(bf16[4,16,2,4,512]{4,3,2,1,0:T(4,128)(2,1)} %broadcast_in_dim.4), calls=%async_computation.1 | async-start | bytes 1048576 | tf_op jit(solution)/shard_map/all_to_all | solution.py:27
  36.1 2.7 %shard_map.175 = (f32[88,128]{1,0:T(8,128)}, bf16[1280,128]{1,0:T(8,128)(2,1)}) custom-call(s32[6]{0:T(128)} %len_ref, f32[2,512]{1,0:T(2,128)} %gain_hbm.1, f32[2,2]{1,0:T(2,128)} %bias_hbm.1, f32[2,2]{1,0:T(2,128)} %rate_hbm.1, bf16[2,4,128]{2,1,0:T(4,128)(2,1)} %taps_hbm.3, bf16[6,3,2,128]{3,2,1,0:T(2,128)(2,1)} %bitcast.45, ...), custom_call_target="tpu_custom_call" | custom-call | tf_op jit(solution)/shard_map/pallas_call | solution.py:536
  38.9 4.1 %all-to-all-done.1 = bf16[4,16,2,4,512]{4,3,2,1,0:T(4,128)(2,1)S(1)} async-done(((bf16[4,16,2,4,512]{4,3,2,1,0:T(4,128)(2,1)}), bf16[4,16,2,4,512]{4,3,2,1,0:T(4,128)(2,1)S(1)}, u32[]{:S(2)}, u32[]{:S(2)}) %all-to-all-start.1) | async-done | bytes 524320 | tf_op jit(solution)/shard_map/all_to_all | solution.py:27
  43.0 1.4 shard_map.176
  44.3 10.7 %all-to-all-start.2 = ((bf16[8,24,640]{2,1,0:T(8,128)(2,1)}), bf16[8,24,640]{2,1,0:T(8,128)(2,1)S(1)}, u32[]{:S(2)}, u32[]{:S(2)}) async-start(bf16[8,24,640]{2,1,0:T(8,128)(2,1)} %shard_map.176), calls=%async_computation.2 | async-start | bytes 491520 | tf_op jit(solution)/shard_map/all_to_all | solution.py:27
  55.0 2.2 %collective-permute-start = (bf16[256,512]{1,0:T(8,128)(2,1)S(1)}, bf16[256,512]{1,0:T(8,128)(2,1)S(1)}, u32[]{:S(2)}, u32[]{:S(2)}) collective-permute-start(bf16[256,512]{1,0:T(8,128)(2,1)S(1)} %bitcast.33), channel_id=1, source_target_pairs={{0,8},{8,16},{16,24},{24,0},{1,9},{9,17},{17,25},{25,1},{2,10},{10... | collective-permute-start | bytes 786440 | tf_op jit(solution)/shard_map/ppermute | solution.py:495
  57.2 3.7 %collective-permute-start.1 = (bf16[256,512]{1,0:T(8,128)(2,1)S(1)}, bf16[256,512]{1,0:T(8,128)(2,1)S(1)}, u32[]{:S(2)}, u32[]{:S(2)}) collective-permute-start(bf16[256,512]{1,0:T(8,128)(2,1)S(1)} %bitcast.34), channel_id=1, source_target_pairs={{0,16},{8,24},{16,0},{24,8},{1,17},{9,25},{17,1},{25,9},{2,18},{10... | collective-permute-start | bytes 786440 | tf_op jit(solution)/shard_map/ppermute | solution.py:495
  60.9 2.5 %collective-permute-start.2 = (bf16[256,512]{1,0:T(8,128)(2,1)S(1)}, bf16[256,512]{1,0:T(8,128)(2,1)S(1)}, u32[]{:S(2)}, u32[]{:S(2)}) collective-permute-start(bf16[256,512]{1,0:T(8,128)(2,1)S(1)} %bitcast.35), channel_id=1, source_target_pairs={{0,24},{8,0},{16,8},{24,16},{1,25},{9,1},{17,9},{25,17},{2,26},{10... | collective-permute-start | bytes 786440 | tf_op jit(solution)/shard_map/ppermute | solution.py:495
  65.3 7.9 %all-to-all-start.3 = ((bf16[32,8,128]{2,1,0:T(8,128)(2,1)}), bf16[32,8,128]{2,1,0:T(8,128)(2,1)S(1)}, u32[]{:S(2)}, u32[]{:S(2)}) async-start(bf16[32,8,128]{2,1,0:T(8,128)(2,1)} %get-tuple-element.36), calls=%async_computation.3 | async-start | bytes 131072 | tf_op jit(solution)/shard_map/all_to_all | solution.py:27
  73.9 6.6 %all-to-all-done.3 = bf16[32,8,128]{2,1,0:T(8,128)(2,1)S(1)} async-done(((bf16[32,8,128]{2,1,0:T(8,128)(2,1)}), bf16[32,8,128]{2,1,0:T(8,128)(2,1)S(1)}, u32[]{:S(2)}, u32[]{:S(2)}) %all-to-all-start.3) | async-done | bytes 65568 | tf_op jit(solution)/shard_map/all_to_all | solution.py:27
  81.3 6.2 %all-to-all-start.4 = ((bf16[16,4,512]{2,1,0:T(4,128)(2,1)}), bf16[16,4,512]{2,1,0:T(4,128)(2,1)S(1)}, u32[]{:S(2)}, u32[]{:S(2)}) async-start(bf16[16,4,512]{2,1,0:T(4,128)(2,1)} %shard_map.179), calls=%async_computation.4 | async-start | bytes 131072 | tf_op jit(solution)/shard_map/all_to_all | solution.py:27
  87.7 2.2 %collective-permute-start.3 = (bf16[1280,128]{1,0:T(8,128)(2,1)S(1)}, bf16[1280,128]{1,0:T(8,128)(2,1)S(1)}, u32[]{:S(2)}, u32[]{:S(2)}) collective-permute-start(bf16[1280,128]{1,0:T(8,128)(2,1)S(1)} %constant_dynamic-update-slice_fusion.w0), channel_id=1, source_target_pairs={{0,8},{8,16},{16,24},{24,0},{1,9},{9,17},{17,25},{25,1},{2,10},{10... | collective-permute-start | bytes 983048 | tf_op jit(solution)/shard_map/ppermute | solution.py:495
  90.0 3.6 %collective-permute-start.4 = (bf16[1280,128]{1,0:T(8,128)(2,1)S(1)}, bf16[1280,128]{1,0:T(8,128)(2,1)S(1)}, u32[]{:S(2)}, u32[]{:S(2)}) collective-permute-start(bf16[1280,128]{1,0:T(8,128)(2,1)S(1)} %constant_dynamic-update-slice_fusion.w0), channel_id=1, source_target_pairs={{0,16},{8,24},{16,0},{24,8},{1,17},{9,25},{17,1},{25,9},{2,18},{10... | collective-permute-start | bytes 983048 | tf_op jit(solution)/shard_map/ppermute | solution.py:495
  93.6 2.9 %collective-permute-start.5 = (bf16[1280,128]{1,0:T(8,128)(2,1)S(1)}, bf16[1280,128]{1,0:T(8,128)(2,1)S(1)}, u32[]{:S(2)}, u32[]{:S(2)}) collective-permute-start(bf16[1280,128]{1,0:T(8,128)(2,1)S(1)} %constant_dynamic-update-slice_fusion.w0), channel_id=1, source_target_pairs={{0,24},{8,0},{16,8},{24,16},{1,25},{9,1},{17,9},{25,17},{2,26},{10... | collective-permute-start | bytes 983048 | tf_op jit(solution)/shard_map/ppermute | solution.py:495
  96.5 2.7 %all-to-all-done.4 = bf16[16,4,512]{2,1,0:T(4,128)(2,1)S(1)} async-done(((bf16[16,4,512]{2,1,0:T(4,128)(2,1)}), bf16[16,4,512]{2,1,0:T(4,128)(2,1)S(1)}, u32[]{:S(2)}, u32[]{:S(2)}) %all-to-all-start.4) | async-done | bytes 65568 | tf_op jit(solution)/shard_map/all_to_all | solution.py:27
  99.3 20.2 %all_to_all.46 = bf16[16,4,512]{2,1,0:T(4,128)(2,1)S(1)} all-to-all(bf16[16,4,512]{2,1,0:T(4,128)(2,1)S(1)} %broadcast_in_dim.5), channel_id=1, replica_groups=mesh['z'=16,'y'=4,'dp'=8] {'z'}, dimensions={0} | all-to-all | bytes 131072 | tf_op jit(solution)/shard_map/all_to_all | solution.py:27
  120.8 7.8 %all-to-all-start.6 = ((bf16[32,8,640]{2,1,0:T(8,128)(2,1)}), bf16[32,8,640]{2,1,0:T(8,128)(2,1)S(1)}, u32[]{:S(2)}, u32[]{:S(2)}) async-start(bf16[32,8,640]{2,1,0:T(8,128)(2,1)} %bitcast.11), calls=%async_computation.6 | async-start | bytes 655360 | tf_op jit(solution)/shard_map/all_to_all | solution.py:27
  129.6 8.4 %all-to-all-done.6 = bf16[32,8,640]{2,1,0:T(8,128)(2,1)S(1)} async-done(((bf16[32,8,640]{2,1,0:T(8,128)(2,1)}), bf16[32,8,640]{2,1,0:T(8,128)(2,1)S(1)}, u32[]{:S(2)}, u32[]{:S(2)}) %all-to-all-start.6) | async-done | bytes 327712 | tf_op jit(solution)/shard_map/all_to_all | solution.py:27
  139.3 3.7 %all-to-all-start.7 = ((bf16[32,8,128]{2,1,0:T(8,128)(2,1)}), bf16[32,8,128]{2,1,0:T(8,128)(2,1)S(1)}, u32[]{:S(2)}, u32[]{:S(2)}) async-start(bf16[32,8,128]{2,1,0:T(8,128)(2,1)} %get-tuple-element.41), calls=%async_computation.7 | async-start | bytes 131072 | tf_op jit(solution)/shard_map/all_to_all | solution.py:27
  144.0 6.4 %all-to-all-done.7 = bf16[32,8,128]{2,1,0:T(8,128)(2,1)S(1)} async-done(((bf16[32,8,128]{2,1,0:T(8,128)(2,1)}), bf16[32,8,128]{2,1,0:T(8,128)(2,1)S(1)}, u32[]{:S(2)}, u32[]{:S(2)}) %all-to-all-start.7) | async-done | bytes 65568 | tf_op jit(solution)/shard_map/all_to_all | solution.py:27
  151.4 3.5 %all-to-all-start.8 = ((bf16[16,4,512]{2,1,0:T(4,128)(2,1)}), bf16[16,4,512]{2,1,0:T(4,128)(2,1)S(1)}, u32[]{:S(2)}, u32[]{:S(2)}) async-start(bf16[16,4,512]{2,1,0:T(4,128)(2,1)} %shard_map.184), calls=%async_computation.8 | async-start | bytes 131072 | tf_op jit(solution)/shard_map/all_to_all | solution.py:27
  155.6 11.1 %all-to-all-done.8.update_ref = bf16[16,4,512]{2,1,0:T(4,128)(2,1)S(1)} async-done(((bf16[16,4,512]{2,1,0:T(4,128)(2,1)}), bf16[16,4,512]{2,1,0:T(4,128)(2,1)S(1)}, u32[]{:S(2)}, u32[]{:S(2)}) %all-to-all-start.8) | async-done | bytes 65568 | tf_op jit(solution)/shard_map/all_to_all | solution.py:27
  (53 shorter events, 11.6 us)
Async XLA Ops:
  31.7 4.3 %copy-start.7 = (bf16[2,512,128]{2,1,0:T(8,128)(2,1)S(1)}, bf16[2,512,128]{2,1,0:T(8,128)(2,1)}, u32[]{:S(2)}) copy-start(bf16[2,512,128]{2,1,0:T(8,128)(2,1)} %param.21) | copy-start | bytes 786436
  31.7 11.2 %all-to-all-start.1 = ((bf16[4,16,2,4,512]{4,3,2,1,0:T(4,128)(2,1)}), bf16[4,16,2,4,512]{4,3,2,1,0:T(4,128)(2,1)S(1)}, u32[]{:S(2)}, u32[]{:S(2)}) async-start(bf16[4,16,2,4,512]{4,3,2,1,0:T(4,128)(2,1)} %broadcast_in_dim.4), calls=%async_computation.1 | async-start | bytes 1048576 | tf_op jit(solution)/shard_map/all_to_all | solution.py:27
  36.1 2.7 %copy-start.5 = (bf16[2,512,128]{2,1,0:T(8,128)(2,1)S(1)}, bf16[2,512,128]{2,1,0:T(8,128)(2,1)}, u32[]{:S(2)}) copy-start(bf16[2,512,128]{2,1,0:T(8,128)(2,1)} %gate_hbm.1) | copy-start | bytes 786436
  36.1 2.7 %copy-start.6 = (bf16[2,512,128]{2,1,0:T(8,128)(2,1)S(1)}, bf16[2,512,128]{2,1,0:T(8,128)(2,1)}, u32[]{:S(2)}) copy-start(bf16[2,512,128]{2,1,0:T(8,128)(2,1)} %value_hbm.1) | copy-start | bytes 786436
  38.8 4.2 %copy-start = (f32[88,128]{1,0:T(8,128)S(1)}, f32[88,128]{1,0:T(8,128)}, u32[]{:S(2)}) copy-start(f32[88,128]{1,0:T(8,128)} %get-tuple-element.33.misc_ref) | copy-start | bytes 135172
  43.0 20.5 %copy-start.3 = (f32[2,6,2,64,128]{4,3,2,1,0:T(8,128)S(1)}, f32[2,6,2,64,128]{4,3,2,1,0:T(8,128)}, u32[]{:S(2)}) copy-start(f32[2,6,2,64,128]{4,3,2,1,0:T(8,128)} %param.27) | copy-start | bytes 2359300
  44.3 10.7 %copy-start.1 = (bf16[2,128,512]{2,1,0:T(8,128)(2,1)S(1)}, bf16[2,128,512]{2,1,0:T(8,128)(2,1)}, u32[]{:S(2)}) copy-start(bf16[2,128,512]{2,1,0:T(8,128)(2,1)} %param.26) | copy-start | bytes 786436
  44.3 19.7 %all-to-all-start.2 = ((bf16[8,24,640]{2,1,0:T(8,128)(2,1)}), bf16[8,24,640]{2,1,0:T(8,128)(2,1)S(1)}, u32[]{:S(2)}, u32[]{:S(2)}) async-start(bf16[8,24,640]{2,1,0:T(8,128)(2,1)} %shard_map.176), calls=%async_computation.2 | async-start | bytes 491520 | tf_op jit(solution)/shard_map/all_to_all | solution.py:27
  55.0 18.1 %collective-permute-start = (bf16[256,512]{1,0:T(8,128)(2,1)S(1)}, bf16[256,512]{1,0:T(8,128)(2,1)S(1)}, u32[]{:S(2)}, u32[]{:S(2)}) collective-permute-start(bf16[256,512]{1,0:T(8,128)(2,1)S(1)} %bitcast.33), channel_id=1, source_target_pairs={{0,8},{8,16},{16,24},{24,0},{1,9},{9,17},{17,25},{25,1},{2,10},{10... | collective-permute-start | bytes 786440 | tf_op jit(solution)/shard_map/ppermute | solution.py:495
  57.2 15.9 %collective-permute-start.1 = (bf16[256,512]{1,0:T(8,128)(2,1)S(1)}, bf16[256,512]{1,0:T(8,128)(2,1)S(1)}, u32[]{:S(2)}, u32[]{:S(2)}) collective-permute-start(bf16[256,512]{1,0:T(8,128)(2,1)S(1)} %bitcast.34), channel_id=1, source_target_pairs={{0,16},{8,24},{16,0},{24,8},{1,17},{9,25},{17,1},{25,9},{2,18},{10... | collective-permute-start | bytes 786440 | tf_op jit(solution)/shard_map/ppermute | solution.py:495
  60.9 12.9 %collective-permute-start.2 = (bf16[256,512]{1,0:T(8,128)(2,1)S(1)}, bf16[256,512]{1,0:T(8,128)(2,1)S(1)}, u32[]{:S(2)}, u32[]{:S(2)}) collective-permute-start(bf16[256,512]{1,0:T(8,128)(2,1)S(1)} %bitcast.35), channel_id=1, source_target_pairs={{0,24},{8,0},{16,8},{24,16},{1,25},{9,1},{17,9},{25,17},{2,26},{10... | collective-permute-start | bytes 786440 | tf_op jit(solution)/shard_map/ppermute | solution.py:495
  65.3 15.2 %all-to-all-start.3 = ((bf16[32,8,128]{2,1,0:T(8,128)(2,1)}), bf16[32,8,128]{2,1,0:T(8,128)(2,1)S(1)}, u32[]{:S(2)}, u32[]{:S(2)}) async-start(bf16[32,8,128]{2,1,0:T(8,128)(2,1)} %get-tuple-element.36), calls=%async_computation.3 | async-start | bytes 131072 | tf_op jit(solution)/shard_map/all_to_all | solution.py:27
  81.3 6.3 %copy-start.2 = (bf16[1280,128]{1,0:T(8,128)(2,1)S(1)}, bf16[1280,128]{1,0:T(8,128)(2,1)}, u32[]{:S(2)}) copy-start(bf16[1280,128]{1,0:T(8,128)(2,1)} %get-tuple-element.39) | copy-start | bytes 983044
  81.3 17.8 %all-to-all-start.4 = ((bf16[16,4,512]{2,1,0:T(4,128)(2,1)}), bf16[16,4,512]{2,1,0:T(4,128)(2,1)S(1)}, u32[]{:S(2)}, u32[]{:S(2)}) async-start(bf16[16,4,512]{2,1,0:T(4,128)(2,1)} %shard_map.179), calls=%async_computation.4 | async-start | bytes 131072 | tf_op jit(solution)/shard_map/all_to_all | solution.py:27
  87.7 11.5 %copy-start.8 = (bf16[3,512]{1,0:T(4,128)(2,1)S(1)}, bf16[3,512]{1,0:T(4,128)(2,1)}, u32[]{:S(2)}) copy-start(bf16[3,512]{1,0:T(4,128)(2,1)} %token_hbm.1) | copy-start | bytes 9220
  87.7 31.8 %collective-permute-start.3 = (bf16[1280,128]{1,0:T(8,128)(2,1)S(1)}, bf16[1280,128]{1,0:T(8,128)(2,1)S(1)}, u32[]{:S(2)}, u32[]{:S(2)}) collective-permute-start(bf16[1280,128]{1,0:T(8,128)(2,1)S(1)} %constant_dynamic-update-slice_fusion.w0), channel_id=1, source_target_pairs={{0,8},{8,16},{16,24},{24,0},{1,9},{9,17},{17,25},{25,1},{2,10},{10... | collective-permute-start | bytes 983048 | tf_op jit(solution)/shard_map/ppermute | solution.py:495
  90.0 29.5 %collective-permute-start.4 = (bf16[1280,128]{1,0:T(8,128)(2,1)S(1)}, bf16[1280,128]{1,0:T(8,128)(2,1)S(1)}, u32[]{:S(2)}, u32[]{:S(2)}) collective-permute-start(bf16[1280,128]{1,0:T(8,128)(2,1)S(1)} %constant_dynamic-update-slice_fusion.w0), channel_id=1, source_target_pairs={{0,16},{8,24},{16,0},{24,8},{1,17},{9,25},{17,1},{25,9},{2,18},{10... | collective-permute-start | bytes 983048 | tf_op jit(solution)/shard_map/ppermute | solution.py:495
  93.6 25.9 %collective-permute-start.5 = (bf16[1280,128]{1,0:T(8,128)(2,1)S(1)}, bf16[1280,128]{1,0:T(8,128)(2,1)S(1)}, u32[]{:S(2)}, u32[]{:S(2)}) collective-permute-start(bf16[1280,128]{1,0:T(8,128)(2,1)S(1)} %constant_dynamic-update-slice_fusion.w0), channel_id=1, source_target_pairs={{0,24},{8,0},{16,8},{24,16},{1,25},{9,1},{17,9},{25,17},{2,26},{10... | collective-permute-start | bytes 983048 | tf_op jit(solution)/shard_map/ppermute | solution.py:495
  120.8 8.8 %copy-start.4 = (f32[2,6,2,64,128]{4,3,2,1,0:T(8,128)S(1)}, f32[2,6,2,64,128]{4,3,2,1,0:T(8,128)}, u32[]{:S(2)}) copy-start(f32[2,6,2,64,128]{4,3,2,1,0:T(8,128)} %param.27) | copy-start | bytes 2359300
  120.8 17.3 %all-to-all-start.6 = ((bf16[32,8,640]{2,1,0:T(8,128)(2,1)}), bf16[32,8,640]{2,1,0:T(8,128)(2,1)S(1)}, u32[]{:S(2)}, u32[]{:S(2)}) async-start(bf16[32,8,640]{2,1,0:T(8,128)(2,1)} %bitcast.11), calls=%async_computation.6 | async-start | bytes 655360 | tf_op jit(solution)/shard_map/all_to_all | solution.py:27
  139.3 11.2 %all-to-all-start.7 = ((bf16[32,8,128]{2,1,0:T(8,128)(2,1)}), bf16[32,8,128]{2,1,0:T(8,128)(2,1)S(1)}, u32[]{:S(2)}, u32[]{:S(2)}) async-start(bf16[32,8,128]{2,1,0:T(8,128)(2,1)} %get-tuple-element.41), calls=%async_computation.7 | async-start | bytes 131072 | tf_op jit(solution)/shard_map/all_to_all | solution.py:27
  151.4 15.2 %all-to-all-start.8 = ((bf16[16,4,512]{2,1,0:T(4,128)(2,1)}), bf16[16,4,512]{2,1,0:T(4,128)(2,1)S(1)}, u32[]{:S(2)}, u32[]{:S(2)}) async-start(bf16[16,4,512]{2,1,0:T(4,128)(2,1)} %shard_map.184), calls=%async_computation.8 | async-start | bytes 131072 | tf_op jit(solution)/shard_map/all_to_all | solution.py:27
where the time goes:
time: 168 us; the launch traced here: 167 us
  starting transfers between devices  61.3 us (36%)
  blocking collectives  48.4 us (29%)
  waiting for transfers between devices  40 us (24%)
  Pallas kernels  14.7 us (9%)
  local copies, waits for them, and re-layouts  1.89 us (1%)
    all_to_all x2, blocking collectives, exchange(): return lax.all_to_all(pieces, axis, 0, 0, tiled=True)  48.4 us
    all_to_all x7, starting transfers between devices, exchange(): return lax.all_to_all(pieces, axis, 0, 0, tiled=True)  44.1 us
    all_to_all x7, waiting for transfers between devices, exchange(): return lax.all_to_all(pieces, axis, 0, 0, tiled=True)  39.3 us
    ppermute x6, starting transfers between devices, from_y(): return lax.ppermute(value, 'y', [(i, (i + k) % YN) for i in range(YN)])  17.2 us
    pallas_call x8, Pallas kernels, call(): pl.pallas_call(kernel, out_shape=outs, in_specs=[vmem] * len(args), out_s...  8.2 us
  transfers between devices with their start and end apart: 13, of which 7 were waited for; matrix products, arithmetic and copies ran while one was open for 1% of the time, Pallas kernels for 4%

commit v1 on v0

--- a/solution.py
+++ b/solution.py
@@ -564,7 +564,7 @@
     later = lax.dynamic_update_slice(base, blocks, (1024, 0))
     vhist, vtaps = call(unpack, [((2, 3, 8, 256), bf16), ((2, 8, 256), bf16)], plane)
 
-    def mid(part, layer, old, *done):
+    def mid(part, layer, pieces, old, *done):
         msg, keep, write, decay, fresh = call(
             functools.partial(middle, layer=layer),
             [
@@ -581,8 +581,9 @@
             old,
         )
         after = close(layer, misc, keep, write, decay, fresh, vhist, old, *done)
+        msg, pieces = lax.optimization_barrier((msg, pieces))
         msg = exchange(msg, ("y", "dp"))
-        return msg.reshape(YN, DN * 8, 128), after
+        return msg.reshape(YN, DN * 8, 128), pieces, after
 
     part = call(
         first_projection,
@@ -594,7 +595,7 @@
     old = recurrent_state[:1]
     part = exchange(part, "dp")
     later_2 = from_y(later, 2)
-    mixed, (state, value0, vector0) = mid(part, 0, old.reshape(1, SEQ, 128, 128))
+    mixed, outs, (state, value0, vector0) = mid(part, 0, outs, old.reshape(1, SEQ, 128, 128))
     later_3 = from_y(later, 3)
     update = call(
         functools.partial(out_projection, first_row=0),
@@ -619,8 +620,9 @@
         step_weight[1:],
         *later,
     )
-    part = exchange(part.reshape(YN * DN, 8, COLS), ("y", "dp")).reshape(YN, DN, 8, COLS)
-    mixed, (state, value1, vector1) = mid(part, 1, old, state)
+    part = exchange(part.reshape(YN * DN, 8, COLS), ("y", "dp"))
+    part = part.reshape(YN, DN, 8, COLS)
+    mixed, outs, (state, value1, vector1) = mid(part, 1, outs, old, state)
     update = call(
         functools.partial(out_projection, first_row=128),
         [((ZN, 4, 512), bf16)],

time: 168 us -> 164 us (0.976)
  blocking collectives: 48.4 us -> 31.5 us
  starting transfers between devices: 61.3 us -> 72.9 us
  local copies, waits for them, and re-layouts: 1.89 us -> 3.65 us
    all_to_all x2, blocking collectives: 48.4 us -> 31.5 us  [exchange(): return lax.all_to_all(pieces, axis, 0, 0, tiled=True)]
    all_to_all x7, starting transfers between devices: 44.1 us -> 53.5 us  [exchange(): return lax.all_to_all(pieces, axis, 0, 0, tiled=True)]
    ppermute x6, starting transfers between devices: 17.2 us -> 19.5 us  [from_y(): return lax.ppermute(value, 'y', [(i, (i + k) % YN) for i in range(YN)])]
    unnamed x19 -> x21, local copies, waits for them, and re-layouts: 0.65 us -> 2.42 us
where the time goes in v1:
time: 164 us; the launch traced here: 163 us
  starting transfers between devices  72.9 us (44%)
  waiting for transfers between devices  39.4 us (24%)
  blocking collectives  31.5 us (19%)
  Pallas kernels  14 us (9%)
  local copies, waits for them, and re-layouts  3.65 us (2%)
    all_to_all x7, starting transfers between devices, exchange(): return lax.all_to_all(pieces, axis, 0, 0, tiled=True)  53.5 us
    all_to_all x7, waiting for transfers between devices, exchange(): return lax.all_to_all(pieces, axis, 0, 0, tiled=True)  39.4 us
    all_to_all x2, blocking collectives, exchange(): return lax.all_to_all(pieces, axis, 0, 0, tiled=True)  31.5 us
    ppermute x6, starting transfers between devices, from_y(): return lax.ppermute(value, 'y', [(i, (i + k) % YN) for i in range(YN)])  19.5 us
    pallas_call x8, Pallas kernels, call(): pl.pallas_call(kernel, out_shape=outs, in_specs=[vmem] * len(args), out_s...  7.58 us
  transfers between devices with their start and end apart: 13, of which 7 were waited for; matrix products, arithmetic and copies ran while one was open for 1% of the time, Pallas kernels for 4%

profile of v1, /device:TPU:1, one launch (start us, length us, event | category | flops | bytes accessed | tf_op | source)
XLA Modules:
  0.0 162.6 jit_solution(654909688581802065)
XLA Ops:
  0.6 1.8 %shard_map.174 = bf16[16,3,4,512]{3,2,1,0:T(4,128)(2,1)} custom-call(bf16[3,512]{1,0:T(4,128)(2,1)} %token_hbm.1, bf16[2,2,32,512]{3,2,1,0:T(8,128)(2,1)} %bitcast.44, bf16[2,6,3,2,32]{4,3,2,1,0:T(2,128)(2,1)} %history_hbm.1, bf16[2,4,2,32]{3,2,1,0:T(2,128)(2,1)} %taps_hbm.2), custom_call_target="tpu_custom_call" | custom-call | tf_op jit(solution)/shard_map/pallas_call | solution.py:515
  2.5 15.9 %all-to-all-start = ((bf16[16,3,4,512]{3,2,1,0:T(4,128)(2,1)}), bf16[16,3,4,512]{3,2,1,0:T(4,128)(2,1)S(1)}, u32[]{:S(2)}, u32[]{:S(2)}) async-start(bf16[16,3,4,512]{3,2,1,0:T(4,128)(2,1)} %shard_map.174), calls=%async_computation | async-start | bytes 393216 | tf_op jit(solution)/shard_map/all_to_all | solution.py:27
  18.4 3.2 %collective-permute-start = (bf16[256,512]{1,0:T(8,128)(2,1)S(1)}, bf16[256,512]{1,0:T(8,128)(2,1)S(1)}, u32[]{:S(2)}, u32[]{:S(2)}) collective-permute-start(bf16[256,512]{1,0:T(8,128)(2,1)S(1)} %bitcast.33), channel_id=1, source_target_pairs={{0,8},{8,16},{16,24},{24,0},{1,9},{9,17},{17,25},{25,1},{2,10},{10... | collective-permute-start | bytes 786440 | tf_op jit(solution)/shard_map/ppermute | solution.py:495
  21.6 4.5 %collective-permute-start.1 = (bf16[256,512]{1,0:T(8,128)(2,1)S(1)}, bf16[256,512]{1,0:T(8,128)(2,1)S(1)}, u32[]{:S(2)}, u32[]{:S(2)}) collective-permute-start(bf16[256,512]{1,0:T(8,128)(2,1)S(1)} %bitcast.34), channel_id=1, source_target_pairs={{0,16},{8,24},{16,0},{24,8},{1,17},{9,25},{17,1},{25,9},{2,18},{10... | collective-permute-start | bytes 786440 | tf_op jit(solution)/shard_map/ppermute | solution.py:495
  26.1 3.0 %collective-permute-start.2 = (bf16[256,512]{1,0:T(8,128)(2,1)S(1)}, bf16[256,512]{1,0:T(8,128)(2,1)S(1)}, u32[]{:S(2)}, u32[]{:S(2)}) collective-permute-start(bf16[256,512]{1,0:T(8,128)(2,1)S(1)} %bitcast.35), channel_id=1, source_target_pairs={{0,24},{8,0},{16,8},{24,16},{1,25},{9,1},{17,9},{25,17},{2,26},{10... | collective-permute-start | bytes 786440 | tf_op jit(solution)/shard_map/ppermute | solution.py:495
  29.1 1.8 %all-to-all-done = bf16[16,3,4,512]{3,2,1,0:T(4,128)(2,1)S(1)} async-done(((bf16[16,3,4,512]{3,2,1,0:T(4,128)(2,1)}), bf16[16,3,4,512]{3,2,1,0:T(4,128)(2,1)S(1)}, u32[]{:S(2)}, u32[]{:S(2)}) %all-to-all-start) | async-done | bytes 196640 | tf_op jit(solution)/shard_map/all_to_all | solution.py:27
  31.9 4.3 %all-to-all-start.1 = ((bf16[4,16,2,4,512]{4,3,2,1,0:T(4,128)(2,1)}), bf16[4,16,2,4,512]{4,3,2,1,0:T(4,128)(2,1)S(1)}, u32[]{:S(2)}, u32[]{:S(2)}) async-start(bf16[4,16,2,4,512]{4,3,2,1,0:T(4,128)(2,1)} %broadcast_in_dim.4), calls=%async_computation.1 | async-start | bytes 1048576 | tf_op jit(solution)/shard_map/all_to_all | solution.py:27
  37.3 2.5 %shard_map.175 = (f32[88,128]{1,0:T(8,128)}, bf16[1280,128]{1,0:T(8,128)(2,1)}) custom-call(s32[6]{0:T(128)} %len_ref, f32[2,512]{1,0:T(2,128)} %gain_hbm.1, f32[2,2]{1,0:T(2,128)} %bias_hbm.1, f32[2,2]{1,0:T(2,128)} %rate_hbm.1, bf16[2,4,128]{2,1,0:T(4,128)(2,1)} %taps_hbm.3, bf16[6,3,2,128]{3,2,1,0:T(2,128)(2,1)} %bitcast.45, ...), custom_call_target="tpu_custom_call" | custom-call | tf_op jit(solution)/shard_map/pallas_call | solution.py:536
  39.8 3.3 %all-to-all-done.1 = bf16[4,16,2,4,512]{4,3,2,1,0:T(4,128)(2,1)S(1)} async-done(((bf16[4,16,2,4,512]{4,3,2,1,0:T(4,128)(2,1)}), bf16[4,16,2,4,512]{4,3,2,1,0:T(4,128)(2,1)S(1)}, u32[]{:S(2)}, u32[]{:S(2)}) %all-to-all-start.1) | async-done | bytes 524320 | tf_op jit(solution)/shard_map/all_to_all | solution.py:27
  45.3 10.6 %all-to-all-start.2 = ((bf16[8,24,640]{2,1,0:T(8,128)(2,1)}), bf16[8,24,640]{2,1,0:T(8,128)(2,1)S(1)}, u32[]{:S(2)}, u32[]{:S(2)}) async-start(bf16[8,24,640]{2,1,0:T(8,128)(2,1)} %shard_map.176), calls=%async_computation.2 | async-start | bytes 491520 | tf_op jit(solution)/shard_map/all_to_all | solution.py:27
  56.4 5.7 %all-to-all-done.2.part_ref = bf16[8,24,640]{2,1,0:T(8,128)(2,1)S(1)} async-done(((bf16[8,24,640]{2,1,0:T(8,128)(2,1)}), bf16[8,24,640]{2,1,0:T(8,128)(2,1)S(1)}, u32[]{:S(2)}, u32[]{:S(2)}) %all-to-all-start.2) | async-done | bytes 245792 | tf_op jit(solution)/shard_map/all_to_all | solution.py:27
  62.7 11.3 %all_to_all.45 = bf16[32,8,128]{2,1,0:T(8,128)(2,1)S(1)} all-to-all(bf16[32,8,128]{2,1,0:T(8,128)(2,1)S(1)} %get-tuple-element.48), channel_id=1, replica_groups=mesh['z'=16,'y'=4,'dp'=8] {'y','dp'}, dimensions={0} | all-to-all | bytes 131072 | tf_op jit(solution)/shard_map/all_to_all | solution.py:27
  74.9 7.7 %all-to-all-start.4 = ((bf16[16,4,512]{2,1,0:T(4,128)(2,1)}), bf16[16,4,512]{2,1,0:T(4,128)(2,1)S(1)}, u32[]{:S(2)}, u32[]{:S(2)}) async-start(bf16[16,4,512]{2,1,0:T(4,128)(2,1)} %shard_map.179), calls=%async_computation.4 | async-start | bytes 131072 | tf_op jit(solution)/shard_map/all_to_all | solution.py:27
  82.8 2.2 %collective-permute-start.3 = (bf16[1280,128]{1,0:T(8,128)(2,1)S(1)}, bf16[1280,128]{1,0:T(8,128)(2,1)S(1)}, u32[]{:S(2)}, u32[]{:S(2)}) collective-permute-start(bf16[1280,128]{1,0:T(8,128)(2,1)S(1)} %constant_dynamic-update-slice_fusion.w0), channel_id=1, source_target_pairs={{0,8},{8,16},{16,24},{24,0},{1,9},{9,17},{17,25},{25,1},{2,10},{10... | collective-permute-start | bytes 983048 | tf_op jit(solution)/shard_map/ppermute | solution.py:495
  85.0 3.6 %collective-permute-start.4 = (bf16[1280,128]{1,0:T(8,128)(2,1)S(1)}, bf16[1280,128]{1,0:T(8,128)(2,1)S(1)}, u32[]{:S(2)}, u32[]{:S(2)}) collective-permute-start(bf16[1280,128]{1,0:T(8,128)(2,1)S(1)} %constant_dynamic-update-slice_fusion.w0), channel_id=1, source_target_pairs={{0,16},{8,24},{16,0},{24,8},{1,17},{9,25},{17,1},{25,9},{2,18},{10... | collective-permute-start | bytes 983048 | tf_op jit(solution)/shard_map/ppermute | solution.py:495
  88.7 2.9 %collective-permute-start.5 = (bf16[1280,128]{1,0:T(8,128)(2,1)S(1)}, bf16[1280,128]{1,0:T(8,128)(2,1)S(1)}, u32[]{:S(2)}, u32[]{:S(2)}) collective-permute-start(bf16[1280,128]{1,0:T(8,128)(2,1)S(1)} %constant_dynamic-update-slice_fusion.w0), channel_id=1, source_target_pairs={{0,24},{8,0},{16,8},{24,16},{1,25},{9,1},{17,9},{25,17},{2,26},{10... | collective-permute-start | bytes 983048 | tf_op jit(solution)/shard_map/ppermute | solution.py:495
  91.6 2.7 %all-to-all-done.4 = bf16[16,4,512]{2,1,0:T(4,128)(2,1)S(1)} async-done(((bf16[16,4,512]{2,1,0:T(4,128)(2,1)}), bf16[16,4,512]{2,1,0:T(4,128)(2,1)S(1)}, u32[]{:S(2)}, u32[]{:S(2)}) %all-to-all-start.4) | async-done | bytes 65568 | tf_op jit(solution)/shard_map/all_to_all | solution.py:27
  94.4 20.2 %all_to_all.46 = bf16[16,4,512]{2,1,0:T(4,128)(2,1)S(1)} all-to-all(bf16[16,4,512]{2,1,0:T(4,128)(2,1)S(1)} %broadcast_in_dim.5), channel_id=1, replica_groups=mesh['z'=16,'y'=4,'dp'=8] {'z'}, dimensions={0} | all-to-all | bytes 131072 | tf_op jit(solution)/shard_map/all_to_all | solution.py:27
  115.9 7.8 %all-to-all-start.6 = ((bf16[32,8,640]{2,1,0:T(8,128)(2,1)}), bf16[32,8,640]{2,1,0:T(8,128)(2,1)S(1)}, u32[]{:S(2)}, u32[]{:S(2)}) async-start(bf16[32,8,640]{2,1,0:T(8,128)(2,1)} %bitcast.11), calls=%async_computation.6 | async-start | bytes 655360 | tf_op jit(solution)/shard_map/all_to_all | solution.py:27
  124.7 8.4 %all-to-all-done.6 = bf16[32,8,640]{2,1,0:T(8,128)(2,1)S(1)} async-done(((bf16[32,8,640]{2,1,0:T(8,128)(2,1)}), bf16[32,8,640]{2,1,0:T(8,128)(2,1)S(1)}, u32[]{:S(2)}, u32[]{:S(2)}) %all-to-all-start.6) | async-done | bytes 327712 | tf_op jit(solution)/shard_map/all_to_all | solution.py:27
  134.4 3.7 %all-to-all-start.7 = ((bf16[32,8,128]{2,1,0:T(8,128)(2,1)}), bf16[32,8,128]{2,1,0:T(8,128)(2,1)S(1)}, u32[]{:S(2)}, u32[]{:S(2)}) async-start(bf16[32,8,128]{2,1,0:T(8,128)(2,1)} %get-tuple-element.57), calls=%async_computation.7 | async-start | bytes 131072 | tf_op jit(solution)/shard_map/all_to_all | solution.py:27
  139.1 6.4 %all-to-all-done.7 = bf16[32,8,128]{2,1,0:T(8,128)(2,1)S(1)} async-done(((bf16[32,8,128]{2,1,0:T(8,128)(2,1)}), bf16[32,8,128]{2,1,0:T(8,128)(2,1)S(1)}, u32[]{:S(2)}, u32[]{:S(2)}) %all-to-all-start.7) | async-done | bytes 65568 | tf_op jit(solution)/shard_map/all_to_all | solution.py:27
  146.5 3.5 %all-to-all-start.8 = ((bf16[16,4,512]{2,1,0:T(4,128)(2,1)}), bf16[16,4,512]{2,1,0:T(4,128)(2,1)S(1)}, u32[]{:S(2)}, u32[]{:S(2)}) async-start(bf16[16,4,512]{2,1,0:T(4,128)(2,1)} %shard_map.184), calls=%async_computation.8 | async-start | bytes 131072 | tf_op jit(solution)/shard_map/all_to_all | solution.py:27
  150.6 11.1 %all-to-all-done.8.update_ref = bf16[16,4,512]{2,1,0:T(4,128)(2,1)S(1)} async-done(((bf16[16,4,512]{2,1,0:T(4,128)(2,1)}), bf16[16,4,512]{2,1,0:T(4,128)(2,1)S(1)}, u32[]{:S(2)}, u32[]{:S(2)}) %all-to-all-start.8) | async-done | bytes 65568 | tf_op jit(solution)/shard_map/all_to_all | solution.py:27
  (55 shorter events, 13.4 us)
Async XLA Ops:
  2.5 15.9 %copy-start.2 = (bf16[2,128,512]{2,1,0:T(8,128)(2,1)S(1)}, bf16[2,128,512]{2,1,0:T(8,128)(2,1)}, u32[]{:S(2)}) copy-start(bf16[2,128,512]{2,1,0:T(8,128)(2,1)} %param.26) | copy-start | bytes 786436
  2.5 28.4 %all-to-all-start = ((bf16[16,3,4,512]{3,2,1,0:T(4,128)(2,1)}), bf16[16,3,4,512]{3,2,1,0:T(4,128)(2,1)S(1)}, u32[]{:S(2)}, u32[]{:S(2)}) async-start(bf16[16,3,4,512]{3,2,1,0:T(4,128)(2,1)} %shard_map.174), calls=%async_computation | async-start | bytes 393216 | tf_op jit(solution)/shard_map/all_to_all | solution.py:27
  18.4 44.3 %collective-permute-start = (bf16[256,512]{1,0:T(8,128)(2,1)S(1)}, bf16[256,512]{1,0:T(8,128)(2,1)S(1)}, u32[]{:S(2)}, u32[]{:S(2)}) collective-permute-start(bf16[256,512]{1,0:T(8,128)(2,1)S(1)} %bitcast.33), channel_id=1, source_target_pairs={{0,8},{8,16},{16,24},{24,0},{1,9},{9,17},{17,25},{25,1},{2,10},{10... | collective-permute-start | bytes 786440 | tf_op jit(solution)/shard_map/ppermute | solution.py:495
  21.6 41.1 %collective-permute-start.1 = (bf16[256,512]{1,0:T(8,128)(2,1)S(1)}, bf16[256,512]{1,0:T(8,128)(2,1)S(1)}, u32[]{:S(2)}, u32[]{:S(2)}) collective-permute-start(bf16[256,512]{1,0:T(8,128)(2,1)S(1)} %bitcast.34), channel_id=1, source_target_pairs={{0,16},{8,24},{16,0},{24,8},{1,17},{9,25},{17,1},{25,9},{2,18},{10... | collective-permute-start | bytes 786440 | tf_op jit(solution)/shard_map/ppermute | solution.py:495
  26.1 36.6 %collective-permute-start.2 = (bf16[256,512]{1,0:T(8,128)(2,1)S(1)}, bf16[256,512]{1,0:T(8,128)(2,1)S(1)}, u32[]{:S(2)}, u32[]{:S(2)}) collective-permute-start(bf16[256,512]{1,0:T(8,128)(2,1)S(1)} %bitcast.35), channel_id=1, source_target_pairs={{0,24},{8,0},{16,8},{24,16},{1,25},{9,1},{17,9},{25,17},{2,26},{10... | collective-permute-start | bytes 786440 | tf_op jit(solution)/shard_map/ppermute | solution.py:495
  31.9 4.3 %copy-start.8 = (bf16[2,512,128]{2,1,0:T(8,128)(2,1)S(1)}, bf16[2,512,128]{2,1,0:T(8,128)(2,1)}, u32[]{:S(2)}) copy-start(bf16[2,512,128]{2,1,0:T(8,128)(2,1)} %param.21) | copy-start | bytes 786436
  31.9 11.2 %all-to-all-start.1 = ((bf16[4,16,2,4,512]{4,3,2,1,0:T(4,128)(2,1)}), bf16[4,16,2,4,512]{4,3,2,1,0:T(4,128)(2,1)S(1)}, u32[]{:S(2)}, u32[]{:S(2)}) async-start(bf16[4,16,2,4,512]{4,3,2,1,0:T(4,128)(2,1)} %broadcast_in_dim.4), calls=%async_computation.1 | async-start | bytes 1048576 | tf_op jit(solution)/shard_map/all_to_all | solution.py:27
  36.2 1.0 copy-start.6
  36.2 1.0 copy-start.7
  43.1 0.8 copy-start
  43.9 11.9 %copy-start.4 = (f32[2,6,2,64,128]{4,3,2,1,0:T(8,128)S(1)}, f32[2,6,2,64,128]{4,3,2,1,0:T(8,128)}, u32[]{:S(2)}) copy-start(f32[2,6,2,64,128]{4,3,2,1,0:T(8,128)} %param.27) | copy-start | bytes 2359300
  45.3 16.9 %all-to-all-start.2 = ((bf16[8,24,640]{2,1,0:T(8,128)(2,1)}), bf16[8,24,640]{2,1,0:T(8,128)(2,1)S(1)}, u32[]{:S(2)}, u32[]{:S(2)}) async-start(bf16[8,24,640]{2,1,0:T(8,128)(2,1)} %shard_map.176), calls=%async_computation.2 | async-start | bytes 491520 | tf_op jit(solution)/shard_map/all_to_all | solution.py:27
  55.9 6.3 %copy-start.1 = (f32[88,128]{1,0:T(8,128)S(1)}, f32[88,128]{1,0:T(8,128)}, u32[]{:S(2)}) copy-start(f32[88,128]{1,0:T(8,128)} %get-tuple-element.43.misc_ref) | copy-start | bytes 135172
  74.9 7.8 %copy-start.3 = (bf16[1280,128]{1,0:T(8,128)(2,1)S(1)}, bf16[1280,128]{1,0:T(8,128)(2,1)}, u32[]{:S(2)}) copy-start(bf16[1280,128]{1,0:T(8,128)(2,1)} %get-tuple-element.54) | copy-start | bytes 983044
  74.9 19.3 %all-to-all-start.4 = ((bf16[16,4,512]{2,1,0:T(4,128)(2,1)}), bf16[16,4,512]{2,1,0:T(4,128)(2,1)S(1)}, u32[]{:S(2)}, u32[]{:S(2)}) async-start(bf16[16,4,512]{2,1,0:T(4,128)(2,1)} %shard_map.179), calls=%async_computation.4 | async-start | bytes 131072 | tf_op jit(solution)/shard_map/all_to_all | solution.py:27
  82.8 11.5 %copy-start.9 = (bf16[3,512]{1,0:T(4,128)(2,1)S(1)}, bf16[3,512]{1,0:T(4,128)(2,1)}, u32[]{:S(2)}) copy-start(bf16[3,512]{1,0:T(4,128)(2,1)} %token_hbm.1) | copy-start | bytes 9220
  82.8 31.8 %collective-permute-start.3 = (bf16[1280,128]{1,0:T(8,128)(2,1)S(1)}, bf16[1280,128]{1,0:T(8,128)(2,1)S(1)}, u32[]{:S(2)}, u32[]{:S(2)}) collective-permute-start(bf16[1280,128]{1,0:T(8,128)(2,1)S(1)} %constant_dynamic-update-slice_fusion.w0), channel_id=1, source_target_pairs={{0,8},{8,16},{16,24},{24,0},{1,9},{9,17},{17,25},{25,1},{2,10},{10... | collective-permute-start | bytes 983048 | tf_op jit(solution)/shard_map/ppermute | solution.py:495
  85.0 29.5 %collective-permute-start.4 = (bf16[1280,128]{1,0:T(8,128)(2,1)S(1)}, bf16[1280,128]{1,0:T(8,128)(2,1)S(1)}, u32[]{:S(2)}, u32[]{:S(2)}) collective-permute-start(bf16[1280,128]{1,0:T(8,128)(2,1)S(1)} %constant_dynamic-update-slice_fusion.w0), channel_id=1, source_target_pairs={{0,16},{8,24},{16,0},{24,8},{1,17},{9,25},{17,1},{25,9},{2,18},{10... | collective-permute-start | bytes 983048 | tf_op jit(solution)/shard_map/ppermute | solution.py:495
  88.7 25.9 %collective-permute-start.5 = (bf16[1280,128]{1,0:T(8,128)(2,1)S(1)}, bf16[1280,128]{1,0:T(8,128)(2,1)S(1)}, u32[]{:S(2)}, u32[]{:S(2)}) collective-permute-start(bf16[1280,128]{1,0:T(8,128)(2,1)S(1)} %constant_dynamic-update-slice_fusion.w0), channel_id=1, source_target_pairs={{0,24},{8,0},{16,8},{24,16},{1,25},{9,1},{17,9},{25,17},{2,26},{10... | collective-permute-start | bytes 983048 | tf_op jit(solution)/shard_map/ppermute | solution.py:495
  115.9 8.8 %copy-start.5 = (f32[2,6,2,64,128]{4,3,2,1,0:T(8,128)S(1)}, f32[2,6,2,64,128]{4,3,2,1,0:T(8,128)}, u32[]{:S(2)}) copy-start(f32[2,6,2,64,128]{4,3,2,1,0:T(8,128)} %param.27) | copy-start | bytes 2359300
  115.9 17.3 %all-to-all-start.6 = ((bf16[32,8,640]{2,1,0:T(8,128)(2,1)}), bf16[32,8,640]{2,1,0:T(8,128)(2,1)S(1)}, u32[]{:S(2)}, u32[]{:S(2)}) async-start(bf16[32,8,640]{2,1,0:T(8,128)(2,1)} %bitcast.11), calls=%async_computation.6 | async-start | bytes 655360 | tf_op jit(solution)/shard_map/all_to_all | solution.py:27
  134.4 11.1 %all-to-all-start.7 = ((bf16[32,8,128]{2,1,0:T(8,128)(2,1)}), bf16[32,8,128]{2,1,0:T(8,128)(2,1)S(1)}, u32[]{:S(2)}, u32[]{:S(2)}) async-start(bf16[32,8,128]{2,1,0:T(8,128)(2,1)} %get-tuple-element.57), calls=%async_computation.7 | async-start | bytes 131072 | tf_op jit(solution)/shard_map/all_to_all | solution.py:27
  146.5 15.2 %all-to-all-start.8 = ((bf16[16,4,512]{2,1,0:T(4,128)(2,1)}), bf16[16,4,512]{2,1,0:T(4,128)(2,1)S(1)}, u32[]{:S(2)}, u32[]{:S(2)}) async-start(bf16[16,4,512]{2,1,0:T(4,128)(2,1)} %shard_map.184), calls=%async_computation.8 | async-start | bytes 131072 | tf_op jit(solution)/shard_map/all_to_all | solution.py:27

commit v2 on v1

--- a/solution.py
+++ b/solution.py
@@ -126,10 +126,10 @@
     if len(rest) == 1:
         rest[0][...] = total.astype(bf16).reshape(ZN, 4, 512)
         return
-    returned_ref, out_ref = rest
-    returned = jnp.concatenate(
-        [returned_ref[:, 0:128], returned_ref[:, 128:256], jnp.zeros((32, 128), bf16)], axis=0
-    )
+    *vector_refs, out_ref = rest
+    old = [ref[k] for ref in vector_refs for k in range(CONV - 1)]
+    returned = [v[:, 0:128].astype(f32) for v in old] + [v[:, 128:256].astype(f32) for v in old]
+    returned = jnp.concatenate([*returned, jnp.zeros((32, 128), f32)], axis=0).astype(bf16)
     slot = one_hot(64, ZN, lambda col: 4 * col + 3)
     halves = []
     for nl in range(2):
@@ -333,7 +333,8 @@
     keep_ref,
     write_ref,
     decay_ref,
-    fresh_ref,
+    value_ref,
+    vector_ref,
     *,
     layer,
 ):
@@ -349,7 +350,6 @@
     squares = jnp.sum(jnp.where(lane == square_lane(), tail, 0.0), axis=1, keepdims=True)
     scaled = (total * lax.rsqrt(squares / D + norm_floor)).astype(bf16)
     rows = mm(place, scaled)
-    fresh_ref[...] = rows[:, 128:512].astype(bf16)
     gate = rows[:, 0:128]
 
     head = 8 * lax.axis_index("z") + 2 * lax.axis_index("y")
@@ -407,20 +407,20 @@
         keep_ref[8 * t : 8 * t + 8] = jnp.exp(cumulative[t] - last) * stepped[t]
         write_ref[8 * t : 8 * t + 8] = write[t]
     decay_ref[...] = jnp.exp(-last)
-
-
-def finish(
-    misc_ref,
-    keep_ref,
-    write_ref,
-    decay_ref,
-    fresh_ref,
-    vhist_ref,
-    state_ref,
-    *rest,
-    layer,
-):
-    next_ref, value_ref, vector_ref = rest[-3:]
+    for out_ref, old, lo, hi in (
+        (value_ref, old_values(misc_ref, layer), 128, 256),
+        (vector_ref, old_vectors(vhist_ref, layer), 256, 512),
+    ):
+        padded = old + [rows[8 * t : 8 * t + 8, lo:hi] for t in range(NEW)]
+        for k in range(CONV - 1):
+            chosen = padded[k + 1]
+            for r in range(k + 2, k + NEW + 1):
+                chosen = jnp.where(lens + k == r, padded[r], chosen)
+            out_ref[k] = chosen.astype(bf16)
+
+
+def finish(keep_ref, write_ref, decay_ref, state_ref, *rest):
+    next_ref = rest[-1]
     kept = jnp.transpose(keep_ref[...])
     _, col = row_col(kept.shape)
     write = write_ref[...].astype(bf16)
@@ -430,17 +430,6 @@
             at = slice(HEAD_DIM * h, HEAD_DIM * h + HEAD_DIM)
             decay = decay_ref[s : s + 1, HEAD_DIM * h : HEAD_DIM * h + 1]
             next_ref[0, s, at] = state_ref[0, s, at] * decay + fresh[at]
-    lens = misc_ref[64:72, 0:1]
-    for out_ref, old, lo, hi in (
-        (value_ref, old_values(misc_ref, layer), 0, 128),
-        (vector_ref, old_vectors(vhist_ref, layer), 128, 384),
-    ):
-        rows = old + [fresh_ref[8 * t : 8 * t + 8, lo:hi].astype(f32) for t in range(NEW)]
-        for k in range(CONV - 1):
-            chosen = rows[k + 1]
-            for r in range(k + 2, k + NEW + 1):
-                chosen = jnp.where(lens + k == r, rows[r], chosen)
-            out_ref[k] = chosen.astype(bf16)
 
 
 def call(kernel, shapes, *args):
@@ -474,19 +463,13 @@
 
 def close(layer, *args):
     vmem = pl.BlockSpec(memory_space=pltpu.VMEM)
-    block = pl.BlockSpec((1, SEQ, 128, 128), lambda i: (layer, 0, 0, 0))
-    space = [vmem] * 7 + [pl.BlockSpec(memory_space=pl.ANY)] * (len(args) - 7)
     return pl.pallas_call(
-        functools.partial(finish, layer=layer),
+        finish,
         grid=(1,),
-        out_shape=[
-            jax.ShapeDtypeStruct((LAYERS, SEQ, 128, 128), f32),
-            jax.ShapeDtypeStruct((3, 8, 128), bf16),
-            jax.ShapeDtypeStruct((3, 8, 256), bf16),
-        ],
-        in_specs=space,
-        out_specs=[block, vmem, vmem],
-        input_output_aliases={7: 0} if layer else {},
+        out_shape=jax.ShapeDtypeStruct((LAYERS, SEQ, 128, 128), f32),
+        in_specs=[vmem] * 4 + [pl.BlockSpec(memory_space=pl.ANY)] * (len(args) - 4),
+        out_specs=pl.BlockSpec((1, SEQ, 128, 128), lambda i: (layer, 0, 0, 0)),
+        input_output_aliases={4: 0} if layer else {},
         compiler_params=pltpu.CompilerParams(vmem_limit_bytes=12 << 20),
     )(*args)
 
@@ -565,14 +548,15 @@
     vhist, vtaps = call(unpack, [((2, 3, 8, 256), bf16), ((2, 8, 256), bf16)], plane)
 
     def mid(part, layer, pieces, old, *done):
-        msg, keep, write, decay, fresh = call(
+        msg, keep, write, decay, value, vector = call(
             functools.partial(middle, layer=layer),
             [
                 ((YN * DN, 8, 128), bf16),
                 ((32, 128), f32),
                 ((32, 128), f32),
                 ((8, 128), f32),
-                ((32, 384), bf16),
+                ((3, 8, 128), bf16),
+                ((3, 8, 256), bf16),
             ],
                         part,
             misc,
@@ -580,10 +564,10 @@
             vtaps,
             old,
         )
-        after = close(layer, misc, keep, write, decay, fresh, vhist, old, *done)
+        after = close(layer, keep, write, decay, old, *done)
         msg, pieces = lax.optimization_barrier((msg, pieces))
         msg = exchange(msg, ("y", "dp"))
-        return msg.reshape(YN, DN * 8, 128), pieces, after
+        return msg.reshape(YN, DN * 8, 128), pieces, (after, value, vector)
 
     part = call(
         first_projection,
@@ -608,9 +592,8 @@
     update = jnp.sum(update.astype(f32), axis=0)[:3]
     token_rows = (tokens.astype(f32) + update).astype(bf16)
     quarter = copies(jnp.pad(token_rows, ((0, 1), (0, 0))), ZN)
-    quarter, old = lax.optimization_barrier((quarter, recurrent_state))
+    quarter, later_state = lax.optimization_barrier((quarter, recurrent_state))
     quarter = exchange(quarter, "z").reshape(64, 512)
-    old = old[1:].reshape(1, SEQ, 128, 128)
     later = [later, later_1, later_2, later_3]
     part = call(
         second_projection,
@@ -622,13 +605,14 @@
     )
     part = exchange(part.reshape(YN * DN, 8, COLS), ("y", "dp"))
     part = part.reshape(YN, DN, 8, COLS)
-    mixed, outs, (state, value1, vector1) = mid(part, 1, outs, old, state)
+    mixed, outs, (state, value1, vector1) = mid(part, 1, outs, later_state[1:].reshape(1, SEQ, 128, 128), state)
     update = call(
         functools.partial(out_projection, first_row=128),
         [((ZN, 4, 512), bf16)],
                 mixed,
         *outs,
-        jnp.concatenate([vector0, vector1], axis=0).reshape(48, 256),
+        vector0,
+        vector1,
     )
     update = exchange(update, "z")
     token_rows, next_vector = call(

time: 164 us -> 162 us (0.988)
  blocking collectives: 31.5 us -> 42.3 us
  waiting for transfers between devices: 39.4 us -> 31 us
  starting transfers between devices: 72.9 us -> 69.1 us
    all_to_all x2 -> x3, blocking collectives: 31.5 us -> 42.3 us  [exchange(): return lax.all_to_all(pieces, axis, 0, 0, tiled=True)]
    all_to_all x7 -> x6, waiting for transfers between devices: 39.4 us -> 31 us  [exchange(): return lax.all_to_all(pieces, axis, 0, 0, tiled=True)]
    all_to_all x7 -> x6, starting transfers between devices: 53.5 us -> 49.6 us  [exchange(): return lax.all_to_all(pieces, axis, 0, 0, tiled=True)]
  transfers between devices with their start and end apart: 13 -> 12, of which waited for: 7 -> 6; matrix products, arithmetic and copies ran while one was open for 1% -> 2% of each run, Pallas kernels for 4% -> 4%
where the time goes in v2:
time: 162 us; the launch traced here: 161 us
  starting transfers between devices  69.1 us (43%)
  blocking collectives  42.3 us (26%)
  waiting for transfers between devices  31 us (19%)
  Pallas kernels  13.4 us (8%)
  local copies, waits for them, and re-layouts  4.65 us (3%)
    all_to_all x6, starting transfers between devices, exchange(): return lax.all_to_all(pieces, axis, 0, 0, tiled=True)  49.6 us
    all_to_all x3, blocking collectives, exchange(): return lax.all_to_all(pieces, axis, 0, 0, tiled=True)  42.3 us
    all_to_all x6, waiting for transfers between devices, exchange(): return lax.all_to_all(pieces, axis, 0, 0, tiled=True)  31 us
    ppermute x6, starting transfers between devices, from_y(): return lax.ppermute(value, 'y', [(i, (i + k) % YN) for i in range(YN)])  19.5 us
    pallas_call x8, Pallas kernels, call(): pl.pallas_call(kernel, out_shape=outs, in_specs=[vmem] * len(args), out_s...  6.93 us
  transfers between devices with their start and end apart: 12, of which 6 were waited for; matrix products, arithmetic and copies ran while one was open for 2% of the time, Pallas kernels for 4%

profile of v2, /device:TPU:1, one launch (start us, length us, event | category | flops | bytes accessed | tf_op | source)
XLA Modules:
  0.0 161.4 jit_solution(11722602386028686947)
XLA Ops:
  0.6 1.8 %shard_map.174 = bf16[16,3,4,512]{3,2,1,0:T(4,128)(2,1)} custom-call(bf16[3,512]{1,0:T(4,128)(2,1)} %token_hbm.1, bf16[2,2,32,512]{3,2,1,0:T(8,128)(2,1)} %bitcast.42, bf16[2,6,3,2,32]{4,3,2,1,0:T(2,128)(2,1)} %history_hbm.1, bf16[2,4,2,32]{3,2,1,0:T(2,128)(2,1)} %taps_hbm.2), custom_call_target="tpu_custom_call" | custom-call | tf_op jit(solution)/shard_map/pallas_call | solution.py:498
  2.5 15.9 %all-to-all-start = ((bf16[16,3,4,512]{3,2,1,0:T(4,128)(2,1)}), bf16[16,3,4,512]{3,2,1,0:T(4,128)(2,1)S(1)}, u32[]{:S(2)}, u32[]{:S(2)}) async-start(bf16[16,3,4,512]{3,2,1,0:T(4,128)(2,1)} %shard_map.174), calls=%async_computation | async-start | bytes 393216 | tf_op jit(solution)/shard_map/all_to_all | solution.py:27
  18.4 3.2 %collective-permute-start = (bf16[256,512]{1,0:T(8,128)(2,1)S(1)}, bf16[256,512]{1,0:T(8,128)(2,1)S(1)}, u32[]{:S(2)}, u32[]{:S(2)}) collective-permute-start(bf16[256,512]{1,0:T(8,128)(2,1)S(1)} %bitcast.31), channel_id=1, source_target_pairs={{0,8},{8,16},{16,24},{24,0},{1,9},{9,17},{17,25},{25,1},{2,10},{10... | collective-permute-start | bytes 786440 | tf_op jit(solution)/shard_map/ppermute | solution.py:478
  21.6 4.5 %collective-permute-start.1 = (bf16[256,512]{1,0:T(8,128)(2,1)S(1)}, bf16[256,512]{1,0:T(8,128)(2,1)S(1)}, u32[]{:S(2)}, u32[]{:S(2)}) collective-permute-start(bf16[256,512]{1,0:T(8,128)(2,1)S(1)} %bitcast.32), channel_id=1, source_target_pairs={{0,16},{8,24},{16,0},{24,8},{1,17},{9,25},{17,1},{25,9},{2,18},{10... | collective-permute-start | bytes 786440 | tf_op jit(solution)/shard_map/ppermute | solution.py:478
  26.1 3.0 %collective-permute-start.2 = (bf16[256,512]{1,0:T(8,128)(2,1)S(1)}, bf16[256,512]{1,0:T(8,128)(2,1)S(1)}, u32[]{:S(2)}, u32[]{:S(2)}) collective-permute-start(bf16[256,512]{1,0:T(8,128)(2,1)S(1)} %bitcast.33), channel_id=1, source_target_pairs={{0,24},{8,0},{16,8},{24,16},{1,25},{9,1},{17,9},{25,17},{2,26},{10... | collective-permute-start | bytes 786440 | tf_op jit(solution)/shard_map/ppermute | solution.py:478
  29.1 1.8 %all-to-all-done = bf16[16,3,4,512]{3,2,1,0:T(4,128)(2,1)S(1)} async-done(((bf16[16,3,4,512]{3,2,1,0:T(4,128)(2,1)}), bf16[16,3,4,512]{3,2,1,0:T(4,128)(2,1)S(1)}, u32[]{:S(2)}, u32[]{:S(2)}) %all-to-all-start) | async-done | bytes 196640 | tf_op jit(solution)/shard_map/all_to_all | solution.py:27
  31.9 4.3 %all-to-all-start.1 = ((bf16[4,16,2,4,512]{4,3,2,1,0:T(4,128)(2,1)}), bf16[4,16,2,4,512]{4,3,2,1,0:T(4,128)(2,1)S(1)}, u32[]{:S(2)}, u32[]{:S(2)}) async-start(bf16[4,16,2,4,512]{4,3,2,1,0:T(4,128)(2,1)} %broadcast_in_dim.4), calls=%async_computation.1 | async-start | bytes 1048576 | tf_op jit(solution)/shard_map/all_to_all | solution.py:27
  37.3 2.5 %shard_map.175 = (f32[88,128]{1,0:T(8,128)}, bf16[1280,128]{1,0:T(8,128)(2,1)}) custom-call(s32[6]{0:T(128)} %len_ref, f32[2,512]{1,0:T(2,128)} %gain_hbm.1, f32[2,2]{1,0:T(2,128)} %bias_hbm.1, f32[2,2]{1,0:T(2,128)} %rate_hbm.1, bf16[2,4,128]{2,1,0:T(4,128)(2,1)} %taps_hbm.3, bf16[6,3,2,128]{3,2,1,0:T(2,128)(2,1)} %bitcast.43, ...), custom_call_target="tpu_custom_call" | custom-call | tf_op jit(solution)/shard_map/pallas_call | solution.py:519
  39.9 3.3 %all-to-all-done.1 = bf16[4,16,2,4,512]{4,3,2,1,0:T(4,128)(2,1)S(1)} async-done(((bf16[4,16,2,4,512]{4,3,2,1,0:T(4,128)(2,1)}), bf16[4,16,2,4,512]{4,3,2,1,0:T(4,128)(2,1)S(1)}, u32[]{:S(2)}, u32[]{:S(2)}) %all-to-all-start.1) | async-done | bytes 524320 | tf_op jit(solution)/shard_map/all_to_all | solution.py:27
  43.9 1.4 shard_map.176
  45.3 10.6 %all-to-all-start.2 = ((bf16[8,24,640]{2,1,0:T(8,128)(2,1)}), bf16[8,24,640]{2,1,0:T(8,128)(2,1)S(1)}, u32[]{:S(2)}, u32[]{:S(2)}) async-start(bf16[8,24,640]{2,1,0:T(8,128)(2,1)} %shard_map.176), calls=%async_computation.2 | async-start | bytes 491520 | tf_op jit(solution)/shard_map/all_to_all | solution.py:27
  56.4 5.7 %all-to-all-done.2.part_ref = bf16[8,24,640]{2,1,0:T(8,128)(2,1)S(1)} async-done(((bf16[8,24,640]{2,1,0:T(8,128)(2,1)}), bf16[8,24,640]{2,1,0:T(8,128)(2,1)S(1)}, u32[]{:S(2)}, u32[]{:S(2)}) %all-to-all-start.2) | async-done | bytes 245792 | tf_op jit(solution)/shard_map/all_to_all | solution.py:27
  62.7 11.3 %all_to_all.45 = bf16[32,8,128]{2,1,0:T(8,128)(2,1)S(1)} all-to-all(bf16[32,8,128]{2,1,0:T(8,128)(2,1)S(1)} %get-tuple-element.44), channel_id=1, replica_groups=mesh['z'=16,'y'=4,'dp'=8] {'y','dp'}, dimensions={0} | all-to-all | bytes 131072 | tf_op jit(solution)/shard_map/all_to_all | solution.py:27
  74.9 7.7 %all-to-all-start.4 = ((bf16[16,4,512]{2,1,0:T(4,128)(2,1)}), bf16[16,4,512]{2,1,0:T(4,128)(2,1)S(1)}, u32[]{:S(2)}, u32[]{:S(2)}) async-start(bf16[16,4,512]{2,1,0:T(4,128)(2,1)} %shard_map.179), calls=%async_computation.4 | async-start | bytes 131072 | tf_op jit(solution)/shard_map/all_to_all | solution.py:27
  82.8 2.2 %collective-permute-start.3 = (bf16[1280,128]{1,0:T(8,128)(2,1)S(1)}, bf16[1280,128]{1,0:T(8,128)(2,1)S(1)}, u32[]{:S(2)}, u32[]{:S(2)}) collective-permute-start(bf16[1280,128]{1,0:T(8,128)(2,1)S(1)} %constant_dynamic-update-slice_fusion.w0), channel_id=1, source_target_pairs={{0,8},{8,16},{16,24},{24,0},{1,9},{9,17},{17,25},{25,1},{2,10},{10... | collective-permute-start | bytes 983048 | tf_op jit(solution)/shard_map/ppermute | solution.py:478
  85.0 3.6 %collective-permute-start.4 = (bf16[1280,128]{1,0:T(8,128)(2,1)S(1)}, bf16[1280,128]{1,0:T(8,128)(2,1)S(1)}, u32[]{:S(2)}, u32[]{:S(2)}) collective-permute-start(bf16[1280,128]{1,0:T(8,128)(2,1)S(1)} %constant_dynamic-update-slice_fusion.w0), channel_id=1, source_target_pairs={{0,16},{8,24},{16,0},{24,8},{1,17},{9,25},{17,1},{25,9},{2,18},{10... | collective-permute-start | bytes 983048 | tf_op jit(solution)/shard_map/ppermute | solution.py:478
  88.7 2.9 %collective-permute-start.5 = (bf16[1280,128]{1,0:T(8,128)(2,1)S(1)}, bf16[1280,128]{1,0:T(8,128)(2,1)S(1)}, u32[]{:S(2)}, u32[]{:S(2)}) collective-permute-start(bf16[1280,128]{1,0:T(8,128)(2,1)S(1)} %constant_dynamic-update-slice_fusion.w0), channel_id=1, source_target_pairs={{0,24},{8,0},{16,8},{24,16},{1,25},{9,1},{17,9},{25,17},{2,26},{10... | collective-permute-start | bytes 983048 | tf_op jit(solution)/shard_map/ppermute | solution.py:478
  91.6 2.7 %all-to-all-done.4 = bf16[16,4,512]{2,1,0:T(4,128)(2,1)S(1)} async-done(((bf16[16,4,512]{2,1,0:T(4,128)(2,1)}), bf16[16,4,512]{2,1,0:T(4,128)(2,1)S(1)}, u32[]{:S(2)}, u32[]{:S(2)}) %all-to-all-start.4) | async-done | bytes 65568 | tf_op jit(solution)/shard_map/all_to_all | solution.py:27
  94.3 20.2 %all_to_all.46 = bf16[16,4,512]{2,1,0:T(4,128)(2,1)S(1)} all-to-all(bf16[16,4,512]{2,1,0:T(4,128)(2,1)S(1)} %broadcast_in_dim.5), channel_id=1, replica_groups=mesh['z'=16,'y'=4,'dp'=8] {'z'}, dimensions={0} | all-to-all | bytes 131072 | tf_op jit(solution)/shard_map/all_to_all | solution.py:27
  115.9 7.7 %all-to-all-start.6 = ((bf16[32,8,640]{2,1,0:T(8,128)(2,1)}), bf16[32,8,640]{2,1,0:T(8,128)(2,1)S(1)}, u32[]{:S(2)}, u32[]{:S(2)}) async-start(bf16[32,8,640]{2,1,0:T(8,128)(2,1)} %bitcast.11), calls=%async_computation.6 | async-start | bytes 655360 | tf_op jit(solution)/shard_map/all_to_all | solution.py:27
  124.6 8.5 %all-to-all-done.6 = bf16[32,8,640]{2,1,0:T(8,128)(2,1)S(1)} async-done(((bf16[32,8,640]{2,1,0:T(8,128)(2,1)}), bf16[32,8,640]{2,1,0:T(8,128)(2,1)S(1)}, u32[]{:S(2)}, u32[]{:S(2)}) %all-to-all-start.6) | async-done | bytes 327712 | tf_op jit(solution)/shard_map/all_to_all | solution.py:27
  133.6 10.8 %all_to_all.47 = bf16[32,8,128]{2,1,0:T(8,128)(2,1)S(1)} all-to-all(bf16[32,8,128]{2,1,0:T(8,128)(2,1)S(1)} %get-tuple-element.53), channel_id=1, replica_groups=mesh['z'=16,'y'=4,'dp'=8] {'y','dp'}, dimensions={0} | all-to-all | bytes 131072 | tf_op jit(solution)/shard_map/all_to_all | solution.py:27
  145.4 3.5 %all-to-all-start.8 = ((bf16[16,4,512]{2,1,0:T(4,128)(2,1)}), bf16[16,4,512]{2,1,0:T(4,128)(2,1)S(1)}, u32[]{:S(2)}, u32[]{:S(2)}) async-start(bf16[16,4,512]{2,1,0:T(4,128)(2,1)} %shard_map.182), calls=%async_computation.8 | async-start | bytes 131072 | tf_op jit(solution)/shard_map/all_to_all | solution.py:27
  151.6 9.1 %all-to-all-done.8.update_ref = bf16[16,4,512]{2,1,0:T(4,128)(2,1)S(1)} async-done(((bf16[16,4,512]{2,1,0:T(4,128)(2,1)}), bf16[16,4,512]{2,1,0:T(4,128)(2,1)S(1)}, u32[]{:S(2)}, u32[]{:S(2)}) %all-to-all-start.8) | async-done | bytes 65568 | tf_op jit(solution)/shard_map/all_to_all | solution.py:27
  (51 shorter events, 12.4 us)
Async XLA Ops:
  2.5 15.9 %copy-start = (bf16[2,128,512]{2,1,0:T(8,128)(2,1)S(1)}, bf16[2,128,512]{2,1,0:T(8,128)(2,1)}, u32[]{:S(2)}) copy-start(bf16[2,128,512]{2,1,0:T(8,128)(2,1)} %param.26) | copy-start | bytes 786436
  2.5 28.4 %all-to-all-start = ((bf16[16,3,4,512]{3,2,1,0:T(4,128)(2,1)}), bf16[16,3,4,512]{3,2,1,0:T(4,128)(2,1)S(1)}, u32[]{:S(2)}, u32[]{:S(2)}) async-start(bf16[16,3,4,512]{3,2,1,0:T(4,128)(2,1)} %shard_map.174), calls=%async_computation | async-start | bytes 393216 | tf_op jit(solution)/shard_map/all_to_all | solution.py:27
  18.4 44.3 %collective-permute-start = (bf16[256,512]{1,0:T(8,128)(2,1)S(1)}, bf16[256,512]{1,0:T(8,128)(2,1)S(1)}, u32[]{:S(2)}, u32[]{:S(2)}) collective-permute-start(bf16[256,512]{1,0:T(8,128)(2,1)S(1)} %bitcast.31), channel_id=1, source_target_pairs={{0,8},{8,16},{16,24},{24,0},{1,9},{9,17},{17,25},{25,1},{2,10},{10... | collective-permute-start | bytes 786440 | tf_op jit(solution)/shard_map/ppermute | solution.py:478
  21.6 41.1 %collective-permute-start.1 = (bf16[256,512]{1,0:T(8,128)(2,1)S(1)}, bf16[256,512]{1,0:T(8,128)(2,1)S(1)}, u32[]{:S(2)}, u32[]{:S(2)}) collective-permute-start(bf16[256,512]{1,0:T(8,128)(2,1)S(1)} %bitcast.32), channel_id=1, source_target_pairs={{0,16},{8,24},{16,0},{24,8},{1,17},{9,25},{17,1},{25,9},{2,18},{10... | collective-permute-start | bytes 786440 | tf_op jit(solution)/shard_map/ppermute | solution.py:478
  26.1 36.6 %collective-permute-start.2 = (bf16[256,512]{1,0:T(8,128)(2,1)S(1)}, bf16[256,512]{1,0:T(8,128)(2,1)S(1)}, u32[]{:S(2)}, u32[]{:S(2)}) collective-permute-start(bf16[256,512]{1,0:T(8,128)(2,1)S(1)} %bitcast.33), channel_id=1, source_target_pairs={{0,24},{8,0},{16,8},{24,16},{1,25},{9,1},{17,9},{25,17},{2,26},{10... | collective-permute-start | bytes 786440 | tf_op jit(solution)/shard_map/ppermute | solution.py:478
  31.9 4.3 %copy-start.7 = (bf16[2,512,128]{2,1,0:T(8,128)(2,1)S(1)}, bf16[2,512,128]{2,1,0:T(8,128)(2,1)}, u32[]{:S(2)}) copy-start(bf16[2,512,128]{2,1,0:T(8,128)(2,1)} %param.21) | copy-start | bytes 786436
  31.9 11.2 %all-to-all-start.1 = ((bf16[4,16,2,4,512]{4,3,2,1,0:T(4,128)(2,1)}), bf16[4,16,2,4,512]{4,3,2,1,0:T(4,128)(2,1)S(1)}, u32[]{:S(2)}, u32[]{:S(2)}) async-start(bf16[4,16,2,4,512]{4,3,2,1,0:T(4,128)(2,1)} %broadcast_in_dim.4), calls=%async_computation.1 | async-start | bytes 1048576 | tf_op jit(solution)/shard_map/all_to_all | solution.py:27
  36.2 1.0 copy-start.5
  36.2 1.0 copy-start.6
  43.1 0.8 copy-start.1
  43.9 11.9 %copy-start.4 = (f32[2,6,2,64,128]{4,3,2,1,0:T(8,128)S(1)}, f32[2,6,2,64,128]{4,3,2,1,0:T(8,128)}, u32[]{:S(2)}) copy-start(f32[2,6,2,64,128]{4,3,2,1,0:T(8,128)} %param.27) | copy-start | bytes 2359300
  45.3 16.9 %all-to-all-start.2 = ((bf16[8,24,640]{2,1,0:T(8,128)(2,1)}), bf16[8,24,640]{2,1,0:T(8,128)(2,1)S(1)}, u32[]{:S(2)}, u32[]{:S(2)}) async-start(bf16[8,24,640]{2,1,0:T(8,128)(2,1)} %shard_map.176), calls=%async_computation.2 | async-start | bytes 491520 | tf_op jit(solution)/shard_map/all_to_all | solution.py:27
  55.9 6.3 %copy-start.2 = (f32[88,128]{1,0:T(8,128)S(1)}, f32[88,128]{1,0:T(8,128)}, u32[]{:S(2)}) copy-start(f32[88,128]{1,0:T(8,128)} %get-tuple-element.39.misc_ref) | copy-start | bytes 135172
  74.9 7.8 %copy-start.3 = (bf16[1280,128]{1,0:T(8,128)(2,1)S(1)}, bf16[1280,128]{1,0:T(8,128)(2,1)}, u32[]{:S(2)}) copy-start(bf16[1280,128]{1,0:T(8,128)(2,1)} %get-tuple-element.50) | copy-start | bytes 983044
  74.9 19.3 %all-to-all-start.4 = ((bf16[16,4,512]{2,1,0:T(4,128)(2,1)}), bf16[16,4,512]{2,1,0:T(4,128)(2,1)S(1)}, u32[]{:S(2)}, u32[]{:S(2)}) async-start(bf16[16,4,512]{2,1,0:T(4,128)(2,1)} %shard_map.179), calls=%async_computation.4 | async-start | bytes 131072 | tf_op jit(solution)/shard_map/all_to_all | solution.py:27
  82.8 11.5 %copy-start.8 = (bf16[3,512]{1,0:T(4,128)(2,1)S(1)}, bf16[3,512]{1,0:T(4,128)(2,1)}, u32[]{:S(2)}) copy-start(bf16[3,512]{1,0:T(4,128)(2,1)} %token_hbm.1) | copy-start | bytes 9220
  82.8 31.8 %collective-permute-start.3 = (bf16[1280,128]{1,0:T(8,128)(2,1)S(1)}, bf16[1280,128]{1,0:T(8,128)(2,1)S(1)}, u32[]{:S(2)}, u32[]{:S(2)}) collective-permute-start(bf16[1280,128]{1,0:T(8,128)(2,1)S(1)} %constant_dynamic-update-slice_fusion.w0), channel_id=1, source_target_pairs={{0,8},{8,16},{16,24},{24,0},{1,9},{9,17},{17,25},{25,1},{2,10},{10... | collective-permute-start | bytes 983048 | tf_op jit(solution)/shard_map/ppermute | solution.py:478
  85.0 29.5 %collective-permute-start.4 = (bf16[1280,128]{1,0:T(8,128)(2,1)S(1)}, bf16[1280,128]{1,0:T(8,128)(2,1)S(1)}, u32[]{:S(2)}, u32[]{:S(2)}) collective-permute-start(bf16[1280,128]{1,0:T(8,128)(2,1)S(1)} %constant_dynamic-update-slice_fusion.w0), channel_id=1, source_target_pairs={{0,16},{8,24},{16,0},{24,8},{1,17},{9,25},{17,1},{25,9},{2,18},{10... | collective-permute-start | bytes 983048 | tf_op jit(solution)/shard_map/ppermute | solution.py:478
  88.7 25.9 %collective-permute-start.5 = (bf16[1280,128]{1,0:T(8,128)(2,1)S(1)}, bf16[1280,128]{1,0:T(8,128)(2,1)S(1)}, u32[]{:S(2)}, u32[]{:S(2)}) collective-permute-start(bf16[1280,128]{1,0:T(8,128)(2,1)S(1)} %constant_dynamic-update-slice_fusion.w0), channel_id=1, source_target_pairs={{0,24},{8,0},{16,8},{24,16},{1,25},{9,1},{17,9},{25,17},{2,26},{10... | collective-permute-start | bytes 983048 | tf_op jit(solution)/shard_map/ppermute | solution.py:478
  115.9 17.2 %all-to-all-start.6 = ((bf16[32,8,640]{2,1,0:T(8,128)(2,1)}), bf16[32,8,640]{2,1,0:T(8,128)(2,1)S(1)}, u32[]{:S(2)}, u32[]{:S(2)}) async-start(bf16[32,8,640]{2,1,0:T(8,128)(2,1)} %bitcast.11), calls=%async_computation.6 | async-start | bytes 655360 | tf_op jit(solution)/shard_map/all_to_all | solution.py:27
  145.4 15.2 %all-to-all-start.8 = ((bf16[16,4,512]{2,1,0:T(4,128)(2,1)}), bf16[16,4,512]{2,1,0:T(4,128)(2,1)S(1)}, u32[]{:S(2)}, u32[]{:S(2)}) async-start(bf16[16,4,512]{2,1,0:T(4,128)(2,1)} %shard_map.182), calls=%async_computation.8 | async-start | bytes 131072 | tf_op jit(solution)/shard_map/all_to_all | solution.py:27

commit v3 on v2

--- a/solution.py
+++ b/solution.py
@@ -447,7 +447,7 @@
 
 def ending(update_ref, token_ref, out_ref, vector_ref):
     total = sum(update_ref[z].astype(f32) for z in range(ZN))
-    out_ref[...] = (total[0:3] + token_ref[...].astype(f32)).astype(bf16)
+    out_ref[...] = (total[0:3] + token_ref[0:3].astype(f32)).astype(bf16)
     rows = [update_ref[z, 3:4, 0:256].astype(f32) for z in range(ZN)]
     rows = jnp.concatenate(rows, axis=0)
     both = jnp.concatenate(
@@ -514,6 +514,8 @@
     )
     first = exchange(first, "z")
     early = jnp.concatenate([gate_weight[0], value_weight[0], step_weight[0]], axis=1)
+    own = jnp.pad(tokens, ((0, 1), (0, 0)))
+    own = lax.optimization_barrier(own)
     out_2 = from_y(outs, 2)
     out_3 = from_y(outs, 3)
     misc, base = pl.pallas_call(
@@ -542,7 +544,7 @@
     )
     plane = exchange(copies(first[:, :2], YN), "y").reshape(128, 4, 512)
     out_1 = from_y(outs, 1)
-    outs = [outs, out_1, out_2, out_3]
+    outs = [outs, out_1, out_2, out_3, own]
     blocks = first[:, 2].reshape(64, 4, 128).transpose(1, 0, 2).reshape(256, 128)
     later = lax.dynamic_update_slice(base, blocks, (1024, 0))
     vhist, vtaps = call(unpack, [((2, 3, 8, 256), bf16), ((2, 8, 256), bf16)], plane)
@@ -580,6 +582,7 @@
     part = exchange(part, "dp")
     later_2 = from_y(later, 2)
     mixed, outs, (state, value0, vector0) = mid(part, 0, outs, old.reshape(1, SEQ, 128, 128))
+    *outs, own = outs
     later_3 = from_y(later, 3)
     update = call(
         functools.partial(out_projection, first_row=0),
@@ -589,9 +592,8 @@
     )
     update = exchange(update, "z")
     later_1 = from_y(later, 1)
-    update = jnp.sum(update.astype(f32), axis=0)[:3]
-    token_rows = (tokens.astype(f32) + update).astype(bf16)
-    quarter = copies(jnp.pad(token_rows, ((0, 1), (0, 0))), ZN)
+    token_rows = (own.astype(f32) + jnp.sum(update.astype(f32), axis=0)).astype(bf16)
+    quarter = copies(token_rows, ZN)
     quarter, later_state = lax.optimization_barrier((quarter, recurrent_state))
     quarter = exchange(quarter, "z").reshape(64, 512)
     later = [later, later_1, later_2, later_3]

time: 162 us -> 162 us (level)
  no operation moved by 1% of the time
where the time goes in v3:
time: 162 us; the launch traced here: 161 us
  starting transfers between devices  69.1 us (43%)
  blocking collectives  42.3 us (26%)
  waiting for transfers between devices  30.3 us (19%)
  Pallas kernels  13.3 us (8%)
  local copies, waits for them, and re-layouts  5.3 us (3%)
    all_to_all x6, starting transfers between devices, exchange(): return lax.all_to_all(pieces, axis, 0, 0, tiled=True)  49.6 us
    all_to_all x3, blocking collectives, exchange(): return lax.all_to_all(pieces, axis, 0, 0, tiled=True)  42.3 us
    all_to_all x6, waiting for transfers between devices, exchange(): return lax.all_to_all(pieces, axis, 0, 0, tiled=True)  30.3 us
    ppermute x6, starting transfers between devices, from_y(): return lax.ppermute(value, 'y', [(i, (i + k) % YN) for i in range(YN)])  19.5 us
    pallas_call x8, Pallas kernels, call(): pl.pallas_call(kernel, out_shape=outs, in_specs=[vmem] * len(args), out_s...  6.92 us
  transfers between devices with their start and end apart: 12, of which 6 were waited for; matrix products, arithmetic and copies ran while one was open for 2% of the time, Pallas kernels for 4%

profile of v3, /device:TPU:1, one launch (start us, length us, event | category | flops | bytes accessed | tf_op | source)
XLA Modules:
  0.0 161.3 jit_solution(6909169749696350410)
XLA Ops:
  0.6 1.8 %shard_map.174 = bf16[16,3,4,512]{3,2,1,0:T(4,128)(2,1)} custom-call(bf16[3,512]{1,0:T(4,128)(2,1)} %token_hbm.1, bf16[2,2,32,512]{3,2,1,0:T(8,128)(2,1)} %bitcast.42, bf16[2,6,3,2,32]{4,3,2,1,0:T(2,128)(2,1)} %history_hbm.1, bf16[2,4,2,32]{3,2,1,0:T(2,128)(2,1)} %taps_hbm.2), custom_call_target="tpu_custom_call" | custom-call | tf_op jit(solution)/shard_map/pallas_call | solution.py:498
  2.5 15.9 %all-to-all-start = ((bf16[16,3,4,512]{3,2,1,0:T(4,128)(2,1)}), bf16[16,3,4,512]{3,2,1,0:T(4,128)(2,1)S(1)}, u32[]{:S(2)}, u32[]{:S(2)}) async-start(bf16[16,3,4,512]{3,2,1,0:T(4,128)(2,1)} %shard_map.174), calls=%async_computation | async-start | bytes 393216 | tf_op jit(solution)/shard_map/all_to_all | solution.py:27
  18.4 3.2 %collective-permute-start = (bf16[256,512]{1,0:T(8,128)(2,1)S(1)}, bf16[256,512]{1,0:T(8,128)(2,1)S(1)}, u32[]{:S(2)}, u32[]{:S(2)}) collective-permute-start(bf16[256,512]{1,0:T(8,128)(2,1)S(1)} %bitcast.31), channel_id=1, source_target_pairs={{0,8},{8,16},{16,24},{24,0},{1,9},{9,17},{17,25},{25,1},{2,10},{10... | collective-permute-start | bytes 786440 | tf_op jit(solution)/shard_map/ppermute | solution.py:478
  21.6 4.5 %collective-permute-start.1 = (bf16[256,512]{1,0:T(8,128)(2,1)S(1)}, bf16[256,512]{1,0:T(8,128)(2,1)S(1)}, u32[]{:S(2)}, u32[]{:S(2)}) collective-permute-start(bf16[256,512]{1,0:T(8,128)(2,1)S(1)} %bitcast.32), channel_id=1, source_target_pairs={{0,16},{8,24},{16,0},{24,8},{1,17},{9,25},{17,1},{25,9},{2,18},{10... | collective-permute-start | bytes 786440 | tf_op jit(solution)/shard_map/ppermute | solution.py:478
  26.1 3.0 %collective-permute-start.2 = (bf16[256,512]{1,0:T(8,128)(2,1)S(1)}, bf16[256,512]{1,0:T(8,128)(2,1)S(1)}, u32[]{:S(2)}, u32[]{:S(2)}) collective-permute-start(bf16[256,512]{1,0:T(8,128)(2,1)S(1)} %bitcast.33), channel_id=1, source_target_pairs={{0,24},{8,0},{16,8},{24,16},{1,25},{9,1},{17,9},{25,17},{2,26},{10... | collective-permute-start | bytes 786440 | tf_op jit(solution)/shard_map/ppermute | solution.py:478
  29.1 1.8 %all-to-all-done = bf16[16,3,4,512]{3,2,1,0:T(4,128)(2,1)S(1)} async-done(((bf16[16,3,4,512]{3,2,1,0:T(4,128)(2,1)}), bf16[16,3,4,512]{3,2,1,0:T(4,128)(2,1)S(1)}, u32[]{:S(2)}, u32[]{:S(2)}) %all-to-all-start) | async-done | bytes 196640 | tf_op jit(solution)/shard_map/all_to_all | solution.py:27
  31.9 4.3 %all-to-all-start.1 = ((bf16[4,16,2,4,512]{4,3,2,1,0:T(4,128)(2,1)}), bf16[4,16,2,4,512]{4,3,2,1,0:T(4,128)(2,1)S(1)}, u32[]{:S(2)}, u32[]{:S(2)}) async-start(bf16[4,16,2,4,512]{4,3,2,1,0:T(4,128)(2,1)} %broadcast_in_dim.4), calls=%async_computation.1 | async-start | bytes 1048576 | tf_op jit(solution)/shard_map/all_to_all | solution.py:27
  37.3 2.5 %shard_map.175 = (f32[88,128]{1,0:T(8,128)}, bf16[1280,128]{1,0:T(8,128)(2,1)}) custom-call(s32[6]{0:T(128)} %len_ref, f32[2,512]{1,0:T(2,128)} %gain_hbm.1, f32[2,2]{1,0:T(2,128)} %bias_hbm.1, f32[2,2]{1,0:T(2,128)} %rate_hbm.1, bf16[2,4,128]{2,1,0:T(4,128)(2,1)} %taps_hbm.3, bf16[6,3,2,128]{3,2,1,0:T(2,128)(2,1)} %bitcast.43, ...), custom_call_target="tpu_custom_call" | custom-call | tf_op jit(solution)/shard_map/pallas_call | solution.py:521
  39.9 3.3 %all-to-all-done.1 = bf16[4,16,2,4,512]{4,3,2,1,0:T(4,128)(2,1)S(1)} async-done(((bf16[4,16,2,4,512]{4,3,2,1,0:T(4,128)(2,1)}), bf16[4,16,2,4,512]{4,3,2,1,0:T(4,128)(2,1)S(1)}, u32[]{:S(2)}, u32[]{:S(2)}) %all-to-all-start.1) | async-done | bytes 524320 | tf_op jit(solution)/shard_map/all_to_all | solution.py:27
  43.9 1.4 shard_map.176
  45.3 10.6 %all-to-all-start.2 = ((bf16[8,24,640]{2,1,0:T(8,128)(2,1)}), bf16[8,24,640]{2,1,0:T(8,128)(2,1)S(1)}, u32[]{:S(2)}, u32[]{:S(2)}) async-start(bf16[8,24,640]{2,1,0:T(8,128)(2,1)} %shard_map.176), calls=%async_computation.2 | async-start | bytes 491520 | tf_op jit(solution)/shard_map/all_to_all | solution.py:27
  57.1 5.1 %all-to-all-done.2.part_ref = bf16[8,24,640]{2,1,0:T(8,128)(2,1)S(1)} async-done(((bf16[8,24,640]{2,1,0:T(8,128)(2,1)}), bf16[8,24,640]{2,1,0:T(8,128)(2,1)S(1)}, u32[]{:S(2)}, u32[]{:S(2)}) %all-to-all-start.2) | async-done | bytes 245792 | tf_op jit(solution)/shard_map/all_to_all | solution.py:27
  62.7 11.3 %all_to_all.45 = bf16[32,8,128]{2,1,0:T(8,128)(2,1)S(1)} all-to-all(bf16[32,8,128]{2,1,0:T(8,128)(2,1)S(1)} %get-tuple-element.46), channel_id=1, replica_groups=mesh['z'=16,'y'=4,'dp'=8] {'y','dp'}, dimensions={0} | all-to-all | bytes 131072 | tf_op jit(solution)/shard_map/all_to_all | solution.py:27
  74.9 7.7 %all-to-all-start.4 = ((bf16[16,4,512]{2,1,0:T(4,128)(2,1)}), bf16[16,4,512]{2,1,0:T(4,128)(2,1)S(1)}, u32[]{:S(2)}, u32[]{:S(2)}) async-start(bf16[16,4,512]{2,1,0:T(4,128)(2,1)} %shard_map.179), calls=%async_computation.4 | async-start | bytes 131072 | tf_op jit(solution)/shard_map/all_to_all | solution.py:27
  82.8 2.2 %collective-permute-start.3 = (bf16[1280,128]{1,0:T(8,128)(2,1)S(1)}, bf16[1280,128]{1,0:T(8,128)(2,1)S(1)}, u32[]{:S(2)}, u32[]{:S(2)}) collective-permute-start(bf16[1280,128]{1,0:T(8,128)(2,1)S(1)} %constant_dynamic-update-slice_fusion.w0), channel_id=1, source_target_pairs={{0,8},{8,16},{16,24},{24,0},{1,9},{9,17},{17,25},{25,1},{2,10},{10... | collective-permute-start | bytes 983048 | tf_op jit(solution)/shard_map/ppermute | solution.py:478
  85.0 3.6 %collective-permute-start.4 = (bf16[1280,128]{1,0:T(8,128)(2,1)S(1)}, bf16[1280,128]{1,0:T(8,128)(2,1)S(1)}, u32[]{:S(2)}, u32[]{:S(2)}) collective-permute-start(bf16[1280,128]{1,0:T(8,128)(2,1)S(1)} %constant_dynamic-update-slice_fusion.w0), channel_id=1, source_target_pairs={{0,16},{8,24},{16,0},{24,8},{1,17},{9,25},{17,1},{25,9},{2,18},{10... | collective-permute-start | bytes 983048 | tf_op jit(solution)/shard_map/ppermute | solution.py:478
  88.7 2.9 %collective-permute-start.5 = (bf16[1280,128]{1,0:T(8,128)(2,1)S(1)}, bf16[1280,128]{1,0:T(8,128)(2,1)S(1)}, u32[]{:S(2)}, u32[]{:S(2)}) collective-permute-start(bf16[1280,128]{1,0:T(8,128)(2,1)S(1)} %constant_dynamic-update-slice_fusion.w0), channel_id=1, source_target_pairs={{0,24},{8,0},{16,8},{24,16},{1,25},{9,1},{17,9},{25,17},{2,26},{10... | collective-permute-start | bytes 983048 | tf_op jit(solution)/shard_map/ppermute | solution.py:478
  91.6 2.7 %all-to-all-done.4 = bf16[16,4,512]{2,1,0:T(4,128)(2,1)S(1)} async-done(((bf16[16,4,512]{2,1,0:T(4,128)(2,1)}), bf16[16,4,512]{2,1,0:T(4,128)(2,1)S(1)}, u32[]{:S(2)}, u32[]{:S(2)}) %all-to-all-start.4) | async-done | bytes 65568 | tf_op jit(solution)/shard_map/all_to_all | solution.py:27
  94.3 20.2 %all_to_all.46 = bf16[16,4,512]{2,1,0:T(4,128)(2,1)S(1)} all-to-all(bf16[16,4,512]{2,1,0:T(4,128)(2,1)S(1)} %broadcast_in_dim.5), channel_id=1, replica_groups=mesh['z'=16,'y'=4,'dp'=8] {'z'}, dimensions={0} | all-to-all | bytes 131072 | tf_op jit(solution)/shard_map/all_to_all | solution.py:27
  115.8 7.7 %all-to-all-start.6 = ((bf16[32,8,640]{2,1,0:T(8,128)(2,1)}), bf16[32,8,640]{2,1,0:T(8,128)(2,1)S(1)}, u32[]{:S(2)}, u32[]{:S(2)}) async-start(bf16[32,8,640]{2,1,0:T(8,128)(2,1)} %bitcast.11), calls=%async_computation.6 | async-start | bytes 655360 | tf_op jit(solution)/shard_map/all_to_all | solution.py:27
  124.5 8.5 %all-to-all-done.6 = bf16[32,8,640]{2,1,0:T(8,128)(2,1)S(1)} async-done(((bf16[32,8,640]{2,1,0:T(8,128)(2,1)}), bf16[32,8,640]{2,1,0:T(8,128)(2,1)S(1)}, u32[]{:S(2)}, u32[]{:S(2)}) %all-to-all-start.6) | async-done | bytes 327712 | tf_op jit(solution)/shard_map/all_to_all | solution.py:27
  133.6 10.8 %all_to_all.47 = bf16[32,8,128]{2,1,0:T(8,128)(2,1)S(1)} all-to-all(bf16[32,8,128]{2,1,0:T(8,128)(2,1)S(1)} %get-tuple-element.55), channel_id=1, replica_groups=mesh['z'=16,'y'=4,'dp'=8] {'y','dp'}, dimensions={0} | all-to-all | bytes 131072 | tf_op jit(solution)/shard_map/all_to_all | solution.py:27
  145.4 3.5 %all-to-all-start.8 = ((bf16[16,4,512]{2,1,0:T(4,128)(2,1)}), bf16[16,4,512]{2,1,0:T(4,128)(2,1)S(1)}, u32[]{:S(2)}, u32[]{:S(2)}) async-start(bf16[16,4,512]{2,1,0:T(4,128)(2,1)} %shard_map.182), calls=%async_computation.8 | async-start | bytes 131072 | tf_op jit(solution)/shard_map/all_to_all | solution.py:27
  151.5 9.0 %all-to-all-done.8.update_ref = bf16[16,4,512]{2,1,0:T(4,128)(2,1)S(1)} async-done(((bf16[16,4,512]{2,1,0:T(4,128)(2,1)}), bf16[16,4,512]{2,1,0:T(4,128)(2,1)S(1)}, u32[]{:S(2)}, u32[]{:S(2)}) %all-to-all-start.8) | async-done | bytes 65568 | tf_op jit(solution)/shard_map/all_to_all | solution.py:27
  (51 shorter events, 13.0 us)
Async XLA Ops:
  2.5 15.9 %copy-start = (bf16[2,128,512]{2,1,0:T(8,128)(2,1)S(1)}, bf16[2,128,512]{2,1,0:T(8,128)(2,1)}, u32[]{:S(2)}) copy-start(bf16[2,128,512]{2,1,0:T(8,128)(2,1)} %param.26) | copy-start | bytes 786436
  2.5 28.4 %all-to-all-start = ((bf16[16,3,4,512]{3,2,1,0:T(4,128)(2,1)}), bf16[16,3,4,512]{3,2,1,0:T(4,128)(2,1)S(1)}, u32[]{:S(2)}, u32[]{:S(2)}) async-start(bf16[16,3,4,512]{3,2,1,0:T(4,128)(2,1)} %shard_map.174), calls=%async_computation | async-start | bytes 393216 | tf_op jit(solution)/shard_map/all_to_all | solution.py:27
  18.4 44.3 %collective-permute-start = (bf16[256,512]{1,0:T(8,128)(2,1)S(1)}, bf16[256,512]{1,0:T(8,128)(2,1)S(1)}, u32[]{:S(2)}, u32[]{:S(2)}) collective-permute-start(bf16[256,512]{1,0:T(8,128)(2,1)S(1)} %bitcast.31), channel_id=1, source_target_pairs={{0,8},{8,16},{16,24},{24,0},{1,9},{9,17},{17,25},{25,1},{2,10},{10... | collective-permute-start | bytes 786440 | tf_op jit(solution)/shard_map/ppermute | solution.py:478
  21.6 41.1 %collective-permute-start.1 = (bf16[256,512]{1,0:T(8,128)(2,1)S(1)}, bf16[256,512]{1,0:T(8,128)(2,1)S(1)}, u32[]{:S(2)}, u32[]{:S(2)}) collective-permute-start(bf16[256,512]{1,0:T(8,128)(2,1)S(1)} %bitcast.32), channel_id=1, source_target_pairs={{0,16},{8,24},{16,0},{24,8},{1,17},{9,25},{17,1},{25,9},{2,18},{10... | collective-permute-start | bytes 786440 | tf_op jit(solution)/shard_map/ppermute | solution.py:478
  26.1 36.6 %collective-permute-start.2 = (bf16[256,512]{1,0:T(8,128)(2,1)S(1)}, bf16[256,512]{1,0:T(8,128)(2,1)S(1)}, u32[]{:S(2)}, u32[]{:S(2)}) collective-permute-start(bf16[256,512]{1,0:T(8,128)(2,1)S(1)} %bitcast.33), channel_id=1, source_target_pairs={{0,24},{8,0},{16,8},{24,16},{1,25},{9,1},{17,9},{25,17},{2,26},{10... | collective-permute-start | bytes 786440 | tf_op jit(solution)/shard_map/ppermute | solution.py:478
  31.9 4.3 %copy-start.7 = (bf16[2,512,128]{2,1,0:T(8,128)(2,1)S(1)}, bf16[2,512,128]{2,1,0:T(8,128)(2,1)}, u32[]{:S(2)}) copy-start(bf16[2,512,128]{2,1,0:T(8,128)(2,1)} %param.21) | copy-start | bytes 786436
  31.9 11.2 %all-to-all-start.1 = ((bf16[4,16,2,4,512]{4,3,2,1,0:T(4,128)(2,1)}), bf16[4,16,2,4,512]{4,3,2,1,0:T(4,128)(2,1)S(1)}, u32[]{:S(2)}, u32[]{:S(2)}) async-start(bf16[4,16,2,4,512]{4,3,2,1,0:T(4,128)(2,1)} %broadcast_in_dim.4), calls=%async_computation.1 | async-start | bytes 1048576 | tf_op jit(solution)/shard_map/all_to_all | solution.py:27
  36.2 1.0 copy-start.5
  36.2 1.0 copy-start.6
  43.1 0.8 copy-start.1
  43.9 11.9 %copy-start.4 = (f32[2,6,2,64,128]{4,3,2,1,0:T(8,128)S(1)}, f32[2,6,2,64,128]{4,3,2,1,0:T(8,128)}, u32[]{:S(2)}) copy-start(f32[2,6,2,64,128]{4,3,2,1,0:T(8,128)} %param.27) | copy-start | bytes 2359300
  45.3 16.9 %all-to-all-start.2 = ((bf16[8,24,640]{2,1,0:T(8,128)(2,1)}), bf16[8,24,640]{2,1,0:T(8,128)(2,1)S(1)}, u32[]{:S(2)}, u32[]{:S(2)}) async-start(bf16[8,24,640]{2,1,0:T(8,128)(2,1)} %shard_map.176), calls=%async_computation.2 | async-start | bytes 491520 | tf_op jit(solution)/shard_map/all_to_all | solution.py:27
  55.8 0.7 copy-start.8
  56.5 5.6 %copy-start.2 = (f32[88,128]{1,0:T(8,128)S(1)}, f32[88,128]{1,0:T(8,128)}, u32[]{:S(2)}) copy-start(f32[88,128]{1,0:T(8,128)} %get-tuple-element.40.misc_ref) | copy-start | bytes 135172
  74.9 7.8 %copy-start.3 = (bf16[1280,128]{1,0:T(8,128)(2,1)S(1)}, bf16[1280,128]{1,0:T(8,128)(2,1)}, u32[]{:S(2)}) copy-start(bf16[1280,128]{1,0:T(8,128)(2,1)} %get-tuple-element.52) | copy-start | bytes 983044
  74.9 19.3 %all-to-all-start.4 = ((bf16[16,4,512]{2,1,0:T(4,128)(2,1)}), bf16[16,4,512]{2,1,0:T(4,128)(2,1)S(1)}, u32[]{:S(2)}, u32[]{:S(2)}) async-start(bf16[16,4,512]{2,1,0:T(4,128)(2,1)} %shard_map.179), calls=%async_computation.4 | async-start | bytes 131072 | tf_op jit(solution)/shard_map/all_to_all | solution.py:27
  82.8 31.7 %collective-permute-start.3 = (bf16[1280,128]{1,0:T(8,128)(2,1)S(1)}, bf16[1280,128]{1,0:T(8,128)(2,1)S(1)}, u32[]{:S(2)}, u32[]{:S(2)}) collective-permute-start(bf16[1280,128]{1,0:T(8,128)(2,1)S(1)} %constant_dynamic-update-slice_fusion.w0), channel_id=1, source_target_pairs={{0,8},{8,16},{16,24},{24,0},{1,9},{9,17},{17,25},{25,1},{2,10},{10... | collective-permute-start | bytes 983048 | tf_op jit(solution)/shard_map/ppermute | solution.py:478
  85.0 29.5 %collective-permute-start.4 = (bf16[1280,128]{1,0:T(8,128)(2,1)S(1)}, bf16[1280,128]{1,0:T(8,128)(2,1)S(1)}, u32[]{:S(2)}, u32[]{:S(2)}) collective-permute-start(bf16[1280,128]{1,0:T(8,128)(2,1)S(1)} %constant_dynamic-update-slice_fusion.w0), channel_id=1, source_target_pairs={{0,16},{8,24},{16,0},{24,8},{1,17},{9,25},{17,1},{25,9},{2,18},{10... | collective-permute-start | bytes 983048 | tf_op jit(solution)/shard_map/ppermute | solution.py:478
  88.7 25.9 %collective-permute-start.5 = (bf16[1280,128]{1,0:T(8,128)(2,1)S(1)}, bf16[1280,128]{1,0:T(8,128)(2,1)S(1)}, u32[]{:S(2)}, u32[]{:S(2)}) collective-permute-start(bf16[1280,128]{1,0:T(8,128)(2,1)S(1)} %constant_dynamic-update-slice_fusion.w0), channel_id=1, source_target_pairs={{0,24},{8,0},{16,8},{24,16},{1,25},{9,1},{17,9},{25,17},{2,26},{10... | collective-permute-start | bytes 983048 | tf_op jit(solution)/shard_map/ppermute | solution.py:478
  115.8 17.2 %all-to-all-start.6 = ((bf16[32,8,640]{2,1,0:T(8,128)(2,1)}), bf16[32,8,640]{2,1,0:T(8,128)(2,1)S(1)}, u32[]{:S(2)}, u32[]{:S(2)}) async-start(bf16[32,8,640]{2,1,0:T(8,128)(2,1)} %bitcast.11), calls=%async_computation.6 | async-start | bytes 655360 | tf_op jit(solution)/shard_map/all_to_all | solution.py:27
  145.4 15.2 %all-to-all-start.8 = ((bf16[16,4,512]{2,1,0:T(4,128)(2,1)}), bf16[16,4,512]{2,1,0:T(4,128)(2,1)S(1)}, u32[]{:S(2)}, u32[]{:S(2)}) async-start(bf16[16,4,512]{2,1,0:T(4,128)(2,1)} %shard_map.182), calls=%async_computation.8 | async-start | bytes 131072 | tf_op jit(solution)/shard_map/all_to_all | solution.py:27
